TPU v7x, 32 devices: a whole 2x2x4 slice. The times are simulated.
32 devices in a mesh: sp: 4 (over z), fs: 4 (over y, x), tp: 2 (over core).
Axes of the slice: x: 2, y: 2, z: 4, core: 2. Of those that a mesh axis runs over, the one named last changes fastest.
Arguments:
- tokens: bfloat16 [4, 1024, 2048], P('fs', 'sp', 'tp'), may hold values from -6 to 6
- norm_gain: float32 [2048], replicated, may hold values from 0.1 to 1.9
- w_query: bfloat16 [2048, 1024], P(('sp', 'fs'), 'tp'), may hold values from -0.125 to 0.125
- forget_weight: bfloat16 [2048, 1024], P(('sp', 'fs'), 'tp'), may hold values from -0.125 to 0.125
- w_input: bfloat16 [2048, 1024], P(('sp', 'fs'), 'tp'), may hold values from -8 to 8
- w_outgate: bfloat16 [2048, 1024], P(('sp', 'fs'), 'tp'), may hold values from -0.125 to 0.125
- w_pool: bfloat16 [2048, 1024], P(('sp', 'fs'), 'tp'), may hold values from -0.125 to 0.125
- forget_gap: float32 [1024], P('tp'), may hold values from 0 to 0.07
- extra_decay: float32 [4, 1024, 8], P('fs', 'sp', 'tp'), may hold values from -0.61 to 0
- rec_gain: float32 [1024], P('tp'), may hold values from 0.1 to 1.9
- group_weight: bfloat16 [4, 256, 256], replicated, may hold values from -0.375 to 0.375
- pool_gain: float32 [1024], P('tp'), may hold values from 0.1 to 1.9
- recurrent_output_weight: bfloat16 [1024, 2048], P('tp', ('sp', 'fs')), may hold values from -0.1875 to 0.1875
- w_out_pool: bfloat16 [1024, 2048], P('tp', ('sp', 'fs')), may hold values from -0.1875 to 0.1875
Outputs:
- mixed_out: bfloat16 [4, 1024, 2048], P('fs', ('sp', 'tp'))
All inputs are finite; a program needn't handle non-finite values.
Results may differ from a plain program's by a relative error of at most 0.011.
Values may be sent and summed in bfloat16 or wider, within the bound.
A program may use at most 64 MiB of HBM per device.

v0:
```python
import jax
import jax.numpy as jnp
from jax import lax
from jax.sharding import PartitionSpec as P

HEAD_DIM = 128
D_HGRN = 1024
POOL_GROUPS = 4
GROUP_DIM = 256
BLOCK = 64


EPS = 1e-06
HIGH = lax.Precision.HIGHEST


def carried_in(x, axis, join, neutral):
    place = lax.axis_index(axis)
    gathered = jax.tree.map(
        lambda a, kind: lax.all_gather(a.astype(kind), axis), x, (jnp.bfloat16, jnp.bfloat16)
    )
    state = jax.tree.map(lambda a, e: jnp.zeros_like(a) + jnp.asarray(e, a.dtype), x, neutral)

    def one(lap, state):
        return join(
            state,
            jax.tree.map(
                lambda a, own: lax.dynamic_index_in_dim(a, lap, 0, False).astype(own.dtype),
                gathered,
                x,
            ),
        )

    return lax.fori_loop(0, place, one, state)


def shifted(x, axis, by):
    peers = lax.axis_size(axis)
    pairs = [(i, i + by) for i in range(peers) if 0 <= i + by < peers]
    return lax.ppermute(x, axis, pairs)


def local_recurrence(queries, input_gate, values, log_forget):
    tok_rows, head_count = (queries.shape[0], queries.shape[1])
    block_count = tok_rows // BLOCK
    q_blk, k_blk, v_blk, g_blk = (
        arr.reshape(block_count, BLOCK, head_count, HEAD_DIM)
        for arr in (queries, input_gate, values, log_forget)
    )
    within = jnp.cumsum(g_blk, axis=1)
    block_end = within[:, -1]
    q_up = q_blk * jnp.exp(within)
    k_down = k_blk * jnp.exp(-within)
    causal = jnp.tril(jnp.ones((BLOCK, BLOCK), jnp.bool_))
    scores = jnp.einsum("nthd,nshd->nhts", q_up, k_down, precision=HIGH)
    scores = jnp.where(causal, scores, 0.0)
    inner_out = jnp.einsum("nhts,nshe->nthe", scores, v_blk, precision=HIGH)
    updates = jnp.einsum(
        "nshd,nshe->nhde", k_blk * jnp.exp(block_end[:, None] - within), v_blk, precision=HIGH
    )
    decays = jnp.exp(block_end)

    def carry_step(carried_state, step_inputs):
        current_shrink_factor, update_now = step_inputs
        return (current_shrink_factor[:, :, None] * carried_state + update_now, carried_state)

    zero_state = jnp.zeros((head_count, HEAD_DIM, HEAD_DIM), jnp.float32)
    final_state, incoming = lax.scan(carry_step, zero_state, (decays, updates))
    local_out = inner_out + jnp.einsum("nthd,nhde->nthe", q_up, incoming, precision=HIGH)
    offsets = jnp.cumsum(block_end, axis=0) - block_end
    total_log = jnp.sum(block_end, axis=0)
    query_dev = q_up * jnp.exp(offsets[:, None])
    return (local_out, final_state, total_log, query_dev)


def combine_states(earlier, later):
    decay_early, state_early = earlier
    decay_late, state_late = later
    return (decay_early * decay_late, decay_late[:, :, None] * state_early + state_late)


def body(
    tokens,
    norm_gain,
    w_query,
    forget_weight,
    w_input,
    w_outgate,
    w_pool,
    forget_gap,
    extra_decay,
    rec_gain,
    group_weight,
    pool_gain,
    recurrent_output_weight,
    w_out_pool,
):
    gathered = lax.all_gather(tokens[0], "tp", axis=1, tiled=True)
    features_f = gathered.astype(jnp.float32)
    token_scale = lax.rsqrt(jnp.mean(features_f * features_f, axis=-1, keepdims=True) + EPS)
    normed = (features_f * token_scale * norm_gain).astype(jnp.bfloat16)
    tok_rows = normed.shape[0]
    width_dev = w_query.shape[1]
    pool_dev = w_pool.shape[1]
    near_rows = (
        lax.all_gather(w_query, "fs", axis=0, tiled=True),
        lax.all_gather(forget_weight, "fs", axis=0, tiled=True),
        lax.all_gather(w_input, "fs", axis=0, tiled=True),
        lax.all_gather(w_outgate, "fs", axis=0, tiled=True),
        lax.all_gather(w_pool, "fs", axis=0, tiled=True),
    )
    full_rows = (
        lax.all_gather(near_rows[0], "sp", axis=0, tiled=True),
        lax.all_gather(near_rows[1], "sp", axis=0, tiled=True),
        lax.all_gather(near_rows[2], "sp", axis=0, tiled=True),
        lax.all_gather(near_rows[3], "sp", axis=0, tiled=True),
        lax.all_gather(near_rows[4], "sp", axis=0, tiled=True),
    )
    z_query, z_forget, z_input, z_outgate, z_pool = (
        jnp.dot(normed, matrix, preferred_element_type=jnp.float32).astype(jnp.bfloat16)
        for matrix in full_rows
    )
    heads_dev = width_dev // HEAD_DIM
    input_gate = forget_gap * jax.nn.sigmoid(-z_forget.astype(jnp.float32))
    log_forget = (
        jnp.log1p(-input_gate).reshape(tok_rows, heads_dev, HEAD_DIM) + extra_decay[0][:, :, None]
    )
    queries = jax.nn.silu(z_query.astype(jnp.float32)).reshape(tok_rows, heads_dev, HEAD_DIM)
    values = z_input.astype(jnp.float32).reshape(tok_rows, heads_dev, HEAD_DIM)
    local_out, end_state, total_log, query_dev = local_recurrence(
        queries, input_gate.reshape(tok_rows, heads_dev, HEAD_DIM), values, log_forget
    )
    identity = (jnp.ones_like(total_log), jnp.zeros_like(end_state))
    scanned = carried_in((jnp.exp(total_log), end_state), "sp", combine_states, identity)
    incoming = scanned[1]
    carried = jnp.einsum("nthd,hde->nthe", query_dev, incoming, precision=HIGH)
    recurrent = (local_out + carried).reshape(tok_rows, width_dev)
    square_sum = lax.psum(jnp.sum(recurrent * recurrent, axis=1), "tp")
    rec_scale = lax.rsqrt(square_sum / D_HGRN + EPS)[:, None]
    recurrent_output = (
        recurrent * rec_scale * rec_gain * jax.nn.silu(z_outgate.astype(jnp.float32))
    ).astype(jnp.bfloat16)
    reach_rows = 2**POOL_GROUPS
    rim_rows = shifted(z_pool[tok_rows - reach_rows :], "sp", 1)
    extended = jnp.concatenate([rim_rows, z_pool], axis=0).astype(jnp.float32)
    running = extended
    window_sums = []
    for level_idx in range(POOL_GROUPS):
        stride = 2**level_idx
        running = running[stride:] + running[:-stride]
        window_sums.append(running[running.shape[0] - tok_rows :])
    groups_dev = pool_dev // GROUP_DIM
    stacked = jnp.stack(window_sums).reshape(POOL_GROUPS, tok_rows, groups_dev, GROUP_DIM)
    group_ids = lax.axis_index("tp") * groups_dev + jnp.arange(groups_dev, dtype=jnp.int32)
    chosen = jnp.arange(POOL_GROUPS, dtype=jnp.int32)[:, None] == group_ids[None, :]
    window_total = jnp.sum(jnp.where(chosen[:, None, :, None], stacked, 0.0), axis=0)
    symbol_indices = lax.axis_index("sp") * tok_rows + jnp.arange(tok_rows, dtype=jnp.int32)
    window_len = jnp.left_shift(jnp.int32(2), group_ids)
    counts_here = jnp.minimum(symbol_indices[:, None] + 1, window_len[None, :]).astype(jnp.float32)
    pooled = (
        window_total / counts_here[:, :, None]
        - z_pool.astype(jnp.float32).reshape(tok_rows, groups_dev, GROUP_DIM)
    ).astype(jnp.bfloat16)
    local_weight = lax.dynamic_slice_in_dim(
        group_weight, lax.axis_index("tp") * groups_dev, groups_dev, 0
    )
    mapped = jnp.einsum("tcd,cde->tce", pooled, local_weight, preferred_element_type=jnp.float32)
    pool_out = (mapped.reshape(tok_rows, pool_dev) * pool_gain).astype(jnp.bfloat16)
    rec_columns, pool_columns = (
        lax.all_gather(recurrent_output_weight, ("sp", "fs"), axis=1, tiled=True),
        lax.all_gather(w_out_pool, ("sp", "fs"), axis=1, tiled=True),
    )
    mixed = lax.psum_scatter(
        (
            jnp.dot(recurrent_output, rec_columns, preferred_element_type=jnp.float32)
            + jnp.dot(pool_out, pool_columns, preferred_element_type=jnp.float32)
        ).astype(jnp.bfloat16),
        "tp",
        scatter_dimension=0,
        tiled=True,
    )
    return mixed[None]


def solution(mesh):
    placed = (
        P("fs", "sp", "tp"),
        P(),
        P(("sp", "fs"), "tp"),
        P(("sp", "fs"), "tp"),
        P(("sp", "fs"), "tp"),
        P(("sp", "fs"), "tp"),
        P(("sp", "fs"), "tp"),
        P("tp"),
        P("fs", "sp", "tp"),
        P("tp"),
        P(),
        P("tp"),
        P("tp", ("sp", "fs")),
        P("tp", ("sp", "fs")),
    )
    return jax.shard_map(
        body, mesh=mesh, in_specs=placed, out_specs=P("fs", ("sp", "tp"), None), check_vma=False
    )
```

profile of v0, /device:TPU:1, one launch (start us, length us, event | category | flops | bytes accessed | tf_op | source)
XLA Modules:
  0.0 406.1 jit_solution(6593802053966810310)
XLA Ops:
  7.3 10.9 %all_gather.54 = bf16[512,512]{1,0:T(8,128)(2,1)} all-gather(bf16[128,512]{1,0:T(8,128)(2,1)} %param.21), channel_id=1, replica_groups=mesh['sp'=4,'fs'=4,'tp'=2] {'fs'}, dimensions={0}, use_global_device_ids=true | all-gather | bytes 655360 | tf_op jit(solution)/shard_map/all_gather | solution.py:107
  18.3 9.0 %all_gather.62 = bf16[512,512]{1,0:T(8,128)(2,1)} all-gather(bf16[128,512]{1,0:T(8,128)(2,1)} %param.24), channel_id=1, replica_groups=mesh['sp'=4,'fs'=4,'tp'=2] {'fs'}, dimensions={0}, use_global_device_ids=true | all-gather | bytes 655360 | tf_op jit(solution)/shard_map/all_gather | solution.py:110
  27.4 8.5 %all_gather.52 = bf16[512,512]{1,0:T(8,128)(2,1)} all-gather(bf16[128,512]{1,0:T(8,128)(2,1)S(1)} %copy-done.6), channel_id=1, replica_groups=mesh['sp'=4,'fs'=4,'tp'=2] {'fs'}, dimensions={0}, use_global_device_ids=true | all-gather | bytes 655360 | tf_op jit(solution)/shard_map/all_gather | solution.py:106
  36.0 9.2 %all_gather.50 = bf16[512,512]{1,0:T(8,128)(2,1)} all-gather(bf16[128,512]{1,0:T(8,128)(2,1)S(1)} %copy-done.7), channel_id=1, replica_groups=mesh['sp'=4,'fs'=4,'tp'=2] {'fs'}, dimensions={0}, use_global_device_ids=true | all-gather | bytes 655360 | tf_op jit(solution)/shard_map/all_gather | solution.py:108
  45.3 9.0 %all_gather.59 = bf16[512,512]{1,0:T(8,128)(2,1)} all-gather(bf16[128,512]{1,0:T(8,128)(2,1)S(1)} %copy-done.8), channel_id=1, replica_groups=mesh['sp'=4,'fs'=4,'tp'=2] {'fs'}, dimensions={0}, use_global_device_ids=true | all-gather | bytes 655360 | tf_op jit(solution)/shard_map/all_gather | solution.py:109
  58.4 9.9 %all-gather.17.cloned.1.call-done = bf16[2048,512]{1,0:T(8,128)(2,1)} async-done(((bf16[512,512]{1,0:T(8,128)(2,1)}), bf16[2048,512]{1,0:T(8,128)(2,1)}) %all-gather.17.cloned.1.call-update) | async-done | bytes 2097168 | tf_op jit(solution)/shard_map/all_gather | solution.py:114
  68.3 2.9 negate_log-plus-one_fusion
  73.5 40.8 %all-gather.23.cloned.1.call-done = bf16[2048,512]{1,0:T(8,128)(2,1)} async-done(((bf16[512,512]{1,0:T(8,128)(2,1)}), bf16[2048,512]{1,0:T(8,128)(2,1)}) %all-gather.23.cloned.1.call-update) | async-done | bytes 2097168 | tf_op jit(solution)/shard_map/all_gather | solution.py:117
  114.3 2.7 convolution_convert_fusion
  120.6 39.6 %all-gather.15.cloned.1.call-done = bf16[2048,512]{1,0:T(8,128)(2,1)} async-done(((bf16[512,512]{1,0:T(8,128)(2,1)}), bf16[2048,512]{1,0:T(8,128)(2,1)}) %all-gather.15.cloned.1.call-update) | async-done | bytes 2097168 | tf_op jit(solution)/shard_map/all_gather | solution.py:113
  160.3 2.4 divide_multiply_fusion
  163.7 42.4 %all-gather.13.cloned.1.call-done = bf16[2048,512]{1,0:T(8,128)(2,1)} async-done(((bf16[512,512]{1,0:T(8,128)(2,1)}), bf16[2048,512]{1,0:T(8,128)(2,1)}) %all-gather.13.cloned.1.call-update) | async-done | bytes 2097168 | tf_op jit(solution)/shard_map/all_gather | solution.py:115
  206.2 2.3 convolution_convert_fusion.4
  213.5 3.7 while.26
  217.2 21.0 %all-gather.2 = bf16[16,128,128]{2,1,0:T(8,128)(2,1)S(1)} all-gather(bf16[4,128,128]{2,1,0:T(8,128)(2,1)S(1)} %convert_element_type.97), channel_id=4, replica_groups=mesh['sp'=4,'fs'=4,'tp'=2] {'sp'}, dimensions={0}, use_global_device_ids=true | all-gather | bytes 655360 | tf_op jit(solution)/shard_map/all_gather | solution.py:20
  238.3 8.3 %all-gather.3 = bf16[4,4,128]{2,1,0:T(4,128)(2,1)S(1)} all-gather(bf16[1,4,128]{2,1,0:T(4,128)(2,1)S(1)} %fusion.42), channel_id=3, replica_groups=mesh['sp'=4,'fs'=4,'tp'=2] {'sp'}, dimensions={0}, use_global_device_ids=true | all-gather | bytes 5120 | tf_op jit(solution)/shard_map/all_gather | solution.py:20
  247.6 2.3 multiply_reduce_fusion
  250.1 5.8 %psum.7 = f32[256]{0:T(256)S(1)} all-reduce(f32[256]{0:T(256)S(1)} %reduce_sum.41), channel_id=1, replica_groups=mesh['sp'=4,'fs'=4,'tp'=2] {'tp'}, use_global_device_ids=true, to_apply=%region_9.10 | all-reduce | flops 256 | bytes 2048 | tf_op jit(solution)/shard_map/psum | solution.py:138
  262.6 2.6 fusion.4
  266.1 58.4 %all-gather.21.cloned.1.call-done = bf16[512,2048]{1,0:T(8,128)(2,1)} async-done(((bf16[512,128]{1,0:T(8,128)(2,1)}), bf16[512,2048]{1,0:T(8,128)(2,1)}) %all-gather.21.cloned.1.call-update) | async-done | bytes 2097168 | tf_op jit(solution)/shard_map/all_gather | solution.py:170
  324.5 4.0 fusion.24
  328.5 59.8 %all-gather.25.cloned.1.call-done = bf16[512,2048]{1,0:T(8,128)(2,1)} async-done(((bf16[512,128]{1,0:T(8,128)(2,1)}), bf16[512,2048]{1,0:T(8,128)(2,1)}) %all-gather.25.cloned.1.call-update) | async-done | bytes 2097168 | tf_op jit(solution)/shard_map/all_gather | solution.py:171
  388.3 3.3 fusion
  391.6 7.9 %reduce-scatter.2.cloned.1.call-done = bf16[128,2048]{1,0:T(8,128)(2,1)} async-done(((bf16[256,2048]{1,0:T(8,128)(2,1)}), bf16[128,2048]{1,0:T(8,128)(2,1)}) %reduce-scatter.2.cloned.1.call-update) | async-done | bytes 524304 | tf_op jit(solution)/shard_map/reduce_scatter | solution.py:173
  (119 shorter events, 29.1 us)
Async XLA Ops:
  6.5 259.1 %copy-start = (bf16[4,256,256]{2,1,0:T(8,128)(2,1)S(1)}, bf16[4,256,256]{2,1,0:T(8,128)(2,1)}, u32[]{:S(2)}) copy-start(bf16[4,256,256]{2,1,0:T(8,128)(2,1)} %param.28) | copy-start | bytes 1572868
  6.5 20.8 %copy-start.6 = (bf16[128,512]{1,0:T(8,128)(2,1)S(1)}, bf16[128,512]{1,0:T(8,128)(2,1)}, u32[]{:S(2)}) copy-start(bf16[128,512]{1,0:T(8,128)(2,1)} %param.20) | copy-start | bytes 393220
  6.5 29.4 %copy-start.7 = (bf16[128,512]{1,0:T(8,128)(2,1)S(1)}, bf16[128,512]{1,0:T(8,128)(2,1)}, u32[]{:S(2)}) copy-start(bf16[128,512]{1,0:T(8,128)(2,1)} %param.22) | copy-start | bytes 393220
  6.5 50.3 %all-gather.27.cloned.1.call-start = ((), (), s32[]{:S(2)}) async-start(), calls=%async_computation.9 | async-start | bytes 1572864 | tf_op jit(solution)/shard_map/all_gather | solution.py:98
  7.3 61.0 %all-gather.17.cloned.1.call-start = ((), (), s32[]{:S(2)}) async-start(), calls=%async_computation.3 | async-start | bytes 2621440 | tf_op jit(solution)/shard_map/all_gather | solution.py:114
  18.2 27.0 %copy-start.8 = (bf16[128,512]{1,0:T(8,128)(2,1)S(1)}, bf16[128,512]{1,0:T(8,128)(2,1)}, u32[]{:S(2)}) copy-start(bf16[128,512]{1,0:T(8,128)(2,1)} %param.23) | copy-start | bytes 393220
  18.2 96.1 %all-gather.23.cloned.1.call-start = ((), (), s32[]{:S(2)}) async-start(), calls=%async_computation.6 | async-start | bytes 2621440 | tf_op jit(solution)/shard_map/all_gather | solution.py:117
  27.3 29.3 %copy-start.10 = (f32[1,256,4]{1,2,0:T(4,128)S(1)}, f32[1,256,4]{1,2,0:T(4,128)}, u32[]{:S(2)}) copy-start(f32[1,256,4]{1,2,0:T(4,128)} %param.26) | copy-start | bytes 12292
  27.3 133.0 %all-gather.15.cloned.1.call-start = ((), (), s32[]{:S(2)}) async-start(), calls=%async_computation.2 | async-start | bytes 2621440 | tf_op jit(solution)/shard_map/all_gather | solution.py:113
  35.9 32.4 %copy-start.15 = (f32[2048]{0:T(1024)S(1)}, f32[2048]{0:T(1024)}, u32[]{:S(2)}) copy-start(f32[2048]{0:T(1024)} %param.19) | copy-start | bytes 24580
  35.9 32.4 %copy-start.17 = (f32[512]{0:T(512)S(1)}, f32[512]{0:T(512)}, u32[]{:S(2)}) copy-start(f32[512]{0:T(512)} %param.25) | copy-start | bytes 6148
  35.9 170.2 %all-gather.13.cloned.1.call-start = ((), (), s32[]{:S(2)}) async-start(), calls=%async_computation.1 | async-start | bytes 2621440 | tf_op jit(solution)/shard_map/all_gather | solution.py:115
  45.2 220.9 %all-gather.19.cloned.1.call-start = ((), (), s32[]{:S(2)}) async-start(), calls=%async_computation.4 | async-start | bytes 2621440 | tf_op jit(solution)/shard_map/all_gather | solution.py:116
  54.3 270.2 %all-gather.21.cloned.1.call-start = ((), (), s32[]{:S(2)}) async-start(), calls=%async_computation.5 | async-start | bytes 2228224 | tf_op jit(solution)/shard_map/all_gather | solution.py:170
  55.0 333.3 %all-gather.25.cloned.1.call-start = ((), (), s32[]{:S(2)}) async-start(), calls=%async_computation.7 | async-start | bytes 2228224 | tf_op jit(solution)/shard_map/all_gather | solution.py:171
  55.8 343.8 %reduce-scatter.2.cloned.1.call-start = ((), (), s32[]{:S(2)}) async-start(), calls=%async_computation.8 | async-start | bytes 1572864 | tf_op jit(solution)/shard_map/reduce_scatter | solution.py:173
  58.3 147.8 %copy-start.12 = (f32[256]{0:T(256)}, f32[256]{0:T(256)S(1)}, u32[]{:S(2)}) copy-start(f32[256]{0:T(256)S(1)} %add_rsqrt_fusion.1) | copy-start | bytes 3076
  73.5 86.7 %copy-start.4 = (bf16[1,256,2048]{2,1,0:T(8,128)(2,1)S(1)}, bf16[1,256,2048]{2,1,0:T(8,128)(2,1)}, u32[]{:S(2)}) copy-start(bf16[1,256,2048]{2,1,0:T(8,128)(2,1)} %all-gather.27.cloned.1.call-done) | copy-start | bytes 3145732
  117.6 139.7 %collective-permute-start = (bf16[16,512]{1,0:T(8,128)(2,1)}, bf16[16,512]{1,0:T(8,128)(2,1)}, u32[]{:S(2)}, u32[]{:S(2)}) collective-permute-start(bf16[16,512]{1,0:T(8,128)(2,1)} %slice.57), channel_id=1, source_target_pairs={{0,8},{8,16},{16,24},{1,9},{9,17},{17,25},{2,10},{10,18},{18,26},{... | collective-permute-start | bytes 49160 | tf_op jit(solution)/shard_map/ppermute | solution.py:40
  213.5 24.8 %copy-start.9 = (f32[4,128]{1,0:T(4,128)S(1)}, f32[4,128]{1,0:T(4,128)}, u32[]{:S(2)}) copy-start(f32[4,128]{1,0:T(4,128)} %get-tuple-element.127) | copy-start | bytes 6148
  258.8 3.8 copy-start.14
  265.2 59.3 %copy-start.5 = (f32[4,64,4,128]{3,2,1,0:T(4,128)S(1)}, f32[4,64,4,128]{3,2,1,0:T(4,128)}, u32[]{:S(2)}) copy-start(f32[4,64,4,128]{3,2,1,0:T(4,128)} %copy.43) | copy-start | bytes 1572868
  265.2 59.3 %copy-start.13 = (f32[256]{0:T(256)S(1)}, f32[256]{0:T(256)}, u32[]{:S(2)}) copy-start(f32[256]{0:T(256)} %copy-done.12) | copy-start | bytes 3076
  265.2 59.2 %copy-start.16 = (f32[2048]{0:T(1024)S(1)}, f32[2048]{0:T(1024)}, u32[]{:S(2)}) copy-start(f32[2048]{0:T(1024)} %param.19) | copy-start | bytes 24580
  (4 other events, 8.5 us)
Sparse Core Ops, SparseCore 0:
  8.9 11.4 all-gather.26
  22.0 46.2 all-gather.16
  69.8 44.4 all-gather.22
  115.8 44.4 all-gather.14
  161.7 44.4 all-gather.12
  207.6 52.9 all-gather.18
  263.3 61.1 all-gather.20
  327.1 61.1 all-gather.24
  391.7 7.7 reduce-scatter.1
where the time goes:
time: 407 us; the launch traced here: 406 us
  waiting for transfers between devices  261 us (64%)
  blocking collectives  81.7 us (20%)
  matrix products  24 us (6%)
  other arithmetic  13.8 us (3%)
  between operations  13.7 us (3%)
  local copies, waits for them, and re-layouts  9.23 us (2%)
    all_gather x1, waiting for transfers between devices, body(): lax.all_gather(w_out_pool, ('sp', 'fs'), axis=1, tiled=True)  59.8 us
    all_gather x1, waiting for transfers between devices, body(): lax.all_gather(recurrent_output_weight, ('sp', 'fs'), axis=1, tiled=True)  58.4 us
    all_gather x1, waiting for transfers between devices, body(): lax.all_gather(near_rows[2], 'sp', axis=0, tiled=True)  42.4 us
    all_gather x1, waiting for transfers between devices, body(): lax.all_gather(near_rows[4], 'sp', axis=0, tiled=True)  40.8 us
    all_gather x1, waiting for transfers between devices, body(): lax.all_gather(near_rows[0], 'sp', axis=0, tiled=True)  39.6 us
    all_gather x2, blocking collectives, carried_in(): lax.all_gather(a.astype(kind), axis)  29.3 us
    all_gather x1, blocking collectives, body(): lax.all_gather(forget_weight, 'fs', axis=0, tiled=True)  10.9 us
    dot_general x4, matrix products, body(): jnp.dot(normed, matrix, preferred_element_type=jnp.float32)  10.3 us
  transfers between devices with their start and end apart: 10, of which 7 were waited for; matrix products, arithmetic and copies ran while one was open for 11% of the time, Pallas kernels for 0%

commit v1 on v0

v1 whole, which is shorter than its diff:
```python
import functools
import jax
import jax.numpy as jnp
from jax import lax
from jax.experimental import pallas as pl
from jax.experimental.pallas import tpu as pltpu
from jax.sharding import PartitionSpec as P

HEAD_DIM = 128
POOL_GROUPS = 4
BLOCK = 64
EPS = 1e-06
HIGH = lax.Precision.HIGHEST
MESH = pl.DeviceIdType.MESH
BF = jnp.bfloat16
F32 = jnp.float32


def place():
    return lax.axis_index("sp"), lax.axis_index("fs"), lax.axis_index("tp")


def rcopy(src, dst, ssem, rsem, dev):
    return pltpu.make_async_remote_copy(
        src_ref=src, dst_ref=dst, send_sem=ssem, recv_sem=rsem, device_id=dev, device_id_type=MESH
    )


def greet(devs):
    barrier = pltpu.get_barrier_semaphore()
    for cond, dev in devs:
        def tell(dev=dev):
            pl.semaphore_signal(barrier, inc=1, device_id=dev, device_id_type=MESH)
        if cond is None:
            tell()
        else:
            pl.when(cond)(tell)
    pl.semaphore_wait(barrier, sum(1 if cond is None else jnp.where(cond, 1, 0) for cond, _ in devs))


def project_kernel(
    n_sp, n_fs, n_tp, tok, wsrc, extra, gain, z_ref, e_ref,
    xs, ws, xs_send, xs_recv, d_send, d_recv, w_send, w_recv, zr_send, zl_send, e_send, e_recv,
):
    s, f, t = place()
    rows, half = tok.shape
    wr = wsrc.shape[1]
    other = (s, f, 1 - t)
    others = [lax.rem(f + d, n_fs) for d in range(1, n_fs)]
    up, down = (s + 1, f, t), (s - 1, f, t)
    has_up, has_down = s < n_sp - 1, s > 0
    greet([(None, other)] + [(None, (s, g, t)) for g in others] + [(has_up, up), (has_down, down)])

    def cols(c):
        return pl.ds(pl.multiple_of(c * half, half), half)

    def slot(a, b):
        return ws.at[pl.ds(pl.multiple_of((a * n_fs + b) * wr, wr), wr), :]

    def to_up(src, a, b):
        return rcopy(src, slot(a, b), zr_send.at[a, b], w_recv.at[a, b], up)

    def to_down(src, a, b):
        return rcopy(src, slot(a, b), zl_send.at[a, b], w_recv.at[a, b], down)

    own = wsrc.at[f]
    w_copies = [rcopy(wsrc.at[g], slot(s, f), w_send.at[d], w_recv.at[s, f], (s, g, t)) for d, g in enumerate(others)]
    for c in w_copies:
        c.start()
    pl.when(has_up)(lambda: to_up(own, s, f).start())
    pl.when(has_down)(lambda: to_down(own, s, f).start())
    x_copies = [rcopy(tok, xs.at[f, :, cols(t)], xs_send.at[d], xs_recv.at[f], (s, g, t)) for d, g in enumerate(others)]
    for c in x_copies:
        c.start()
    e_copies = [rcopy(extra.at[g], e_ref.at[f], e_send.at[d], e_recv.at[f], (s, g, t)) for d, g in enumerate(others)]
    for c in e_copies:
        c.start()
    first = rcopy(tok, xs.at[f, :, cols(t)], d_send.at[f], d_recv.at[f], other)
    first.start()
    ws[pl.ds(pl.multiple_of((s * n_fs + f) * wr, wr), wr), :] = wsrc[f]
    xs[f, :, cols(t)] = tok[...]
    e_ref[f] = extra[f]

    for g in others:
        to_up(slot(s, g), s, g).wait_recv()
        pl.when(has_up)(lambda: to_up(slot(s, g), s, g).start())
        pl.when(has_down)(lambda: to_down(slot(s, g), s, g).start())

    def swap(g):
        part = xs.at[g, :, cols(t)]
        return rcopy(part, part, d_send.at[g], d_recv.at[g], other)

    order = [f] + others

    def relay(d):
        for g in order:
            a = s - d

            @pl.when(a >= 0)
            def _():
                to_up(slot(a, g), a, g).wait_recv()
                pl.when(has_up)(lambda: to_up(slot(a, g), a, g).start())
            b = s + d

            @pl.when(b < n_sp)
            def _():
                to_down(slot(b, g), b, g).wait_recv()
                pl.when(has_down)(lambda: to_down(slot(b, g), b, g).start())

    def norm(g):
        theirs = xs.at[g, :, cols(1 - t)]
        rcopy(theirs, theirs, d_send.at[g], d_recv.at[g], other).wait_recv()
        step = 32
        for i in range(rows // step):
            feats = xs[g, pl.ds(i * step, step), :].astype(F32)
            scale = lax.rsqrt(jnp.mean(feats * feats, axis=-1, keepdims=True) + EPS)
            xs[g, pl.ds(i * step, step), :] = (feats * scale * gain[...]).astype(BF)

    relay(1)
    for i, g in enumerate(others):
        part = xs.at[g, :, cols(t)]
        rcopy(part, part, xs_send.at[i], xs_recv.at[g], other).wait_recv()
        swap(g).start()
    for d in range(2, n_sp):
        relay(d)
    for c in w_copies + x_copies + e_copies:
        c.wait_send()
    for g in others:
        rcopy(extra.at[f], e_ref.at[g], e_send.at[0], e_recv.at[g], other).wait_recv()
    first.wait_send()
    for g in others:
        swap(g).wait_send()
    for g in order:
        norm(g)

    def each(i, _):
        z_ref[i] = jnp.dot(xs[i], ws[...], preferred_element_type=F32).astype(BF)
        return 0

    lax.fori_loop(0, n_fs, each, 0)

    for d in range(n_sp):
        for g in order:
            a = s - d

            @pl.when((a >= 0) & has_up)
            def _():
                to_up(slot(a, g), a, g).wait_send()
            b = s + d

            @pl.when((b < n_sp) & has_down)
            def _():
                to_down(slot(b, g), b, g).wait_send()


def state_kernel(n_sp, state, decay, edge, st_out, de_out, ed_out, s_send, s_recv, c_send, c_recv, g_send, g_recv):
    s, f, t = place()
    devs = []
    for d in range(1, n_sp):
        devs.append((s + d < n_sp, (s + d, f, t)))
        devs.append((s - d >= 0, (s - d, f, t)))
    greet(devs)
    nxt = (s + 1, f, t)
    edge_copy = rcopy(edge, ed_out, g_send, g_recv, nxt)
    pl.when(s < n_sp - 1)(edge_copy.start)

    def pair(d):
        dev = (s + d, f, t)
        return (
            rcopy(state, st_out.at[d - 1], s_send.at[d - 1], s_recv.at[d - 1], dev),
            rcopy(decay, de_out.at[d - 1], c_send.at[d - 1], c_recv.at[d - 1], dev),
        )

    for d in range(1, n_sp):
        @pl.when(s + d < n_sp)
        def _():
            for c in pair(d):
                c.start()
    pl.when(s == 0)(lambda: ed_out.__setitem__(Ellipsis, jnp.zeros(ed_out.shape, ed_out.dtype)))
    for d in range(1, n_sp):
        @pl.when(s - d < 0)
        def _():
            st_out[d - 1] = jnp.zeros(st_out.shape[1:], st_out.dtype)
            de_out[d - 1] = jnp.ones(de_out.shape[1:], de_out.dtype)
    for d in range(1, n_sp):
        @pl.when(s - d >= 0)
        def _():
            for c in pair(d):
                c.wait_recv()
        @pl.when(s + d < n_sp)
        def _():
            for c in pair(d):
                c.wait_send()
    pl.when(s < n_sp - 1)(edge_copy.wait_send)
    pl.when(s > 0)(edge_copy.wait_recv)


def mix_kernel(
    n_sp, n_fs, n_tp, rec, pool, sq, ow, a_rec, a_pool, sq_out, ow_out,
    relay_buf, r_send, r_recv, p_send, p_recv, q_send, q_recv, dr_send, dr_recv, dp_send, dp_recv,
    up_send, down_send, o_recv, od_send, od_recv,
):
    s, f, t = place()
    n_half = n_sp // n_tp
    other = (s, f, 1 - t)
    others = [lax.rem(f + d, n_fs) for d in range(1, n_fs)]
    up, down = (s + 1, f, t), (s - 1, f, t)
    has_up, has_down = s < n_sp - 1, s > 0
    greet(
        [(None, other)] + [(None, (s, g, u)) for g in others for u in (t, 1 - t)] + [(has_up, up), (has_down, down)]
    )

    def cols(g, u):
        return pl.ds(pl.multiple_of((u * n_fs + g) * HEAD_DIM, HEAD_DIM), HEAD_DIM)

    def to_up(src, a):
        return rcopy(src, relay_buf.at[a], up_send.at[a], o_recv.at[a], up)

    def to_down(src, a):
        return rcopy(src, relay_buf.at[a], down_send.at[a], o_recv.at[a], down)

    def to_other(src, a):
        return rcopy(src, ow_out.at[lax.rem(a, n_half), t], od_send.at[a], od_recv.at[a], other)

    def keep(src, a):
        mine = a // n_half == t

        @pl.when(mine)
        def _():
            ow_out[lax.rem(a, n_half), t] = src[...]

        pl.when(jnp.logical_not(mine))(lambda: to_other(src, a).start())

    pl.when(has_up)(lambda: to_up(ow, s).start())
    pl.when(has_down)(lambda: to_down(ow, s).start())
    sends = []
    for d, g in enumerate(others):
        sends.append(rcopy(pool, a_pool.at[:, cols(f, t)], p_send.at[d], p_recv.at[f], (s, g, t)))
        sends.append(rcopy(rec, a_rec.at[:, cols(f, t)], r_send.at[d], r_recv.at[f], (s, g, t)))
        for u in range(n_tp):
            sends.append(rcopy(sq, sq_out.at[t, f], q_send.at[u, d], q_recv.at[t, f], (s, g, u)))
    sends.append(rcopy(pool, a_pool.at[:, cols(f, t)], dp_send.at[f], dp_recv.at[f], other))
    sends.append(rcopy(rec, a_rec.at[:, cols(f, t)], dr_send.at[f], dr_recv.at[f], other))
    sends.append(rcopy(sq, sq_out.at[t, f], q_send.at[0, n_fs - 1], q_recv.at[t, f], other))
    for c in sends:
        c.start()
    a_pool[:, cols(f, t)] = pool[...]
    a_rec[:, cols(f, t)] = rec[...]
    sq_out[t, f] = sq[...]
    keep(ow, s)
    for d, g in enumerate(others):
        for arr, rs, ds_, dr in ((a_pool, p_recv, dp_send, dp_recv), (a_rec, r_recv, dr_send, dr_recv)):
            part = arr.at[:, cols(g, t)]
            rcopy(part, part, ds_.at[g], rs.at[g], other).wait_recv()
            c = rcopy(part, part, ds_.at[g], dr.at[g], other)
            c.start()
            sends.append(c)
    for d in range(1, n_sp):
        a = s - d

        @pl.when(a >= 0)
        def _():
            to_up(relay_buf.at[a], a).wait_recv()
            pl.when(has_up)(lambda: to_up(relay_buf.at[a], a).start())
            keep(relay_buf.at[a], a)
        b = s + d

        @pl.when(b < n_sp)
        def _():
            to_down(relay_buf.at[b], b).wait_recv()
            pl.when(has_down)(lambda: to_down(relay_buf.at[b], b).start())
            keep(relay_buf.at[b], b)
    for g in [f] + others:
        for arr, ds_, dr in ((a_pool, dp_send, dp_recv), (a_rec, dr_send, dr_recv)):
            part = arr.at[:, cols(g, 1 - t)]
            rcopy(part, part, ds_.at[g], dr.at[g], other).wait_recv()
        for u in range(n_tp):
            here = sq_out.at[u, g]
            needed = rcopy(here, here, q_send.at[0, 0], q_recv.at[u, g], other)
            pl.when(jnp.logical_or(g != f, u != t))(needed.wait_recv)
    for i in range(n_half):
        a = t * n_half + i
        here = ow_out.at[i, 1 - t]
        rcopy(here, here, od_send.at[a], od_recv.at[a], other).wait_recv()
    for c in sends:
        c.wait_send()
    for i in range(n_half):
        a = (1 - t) * n_half + i
        to_other(ow, a).wait_send()
    for d in range(n_sp):
        a, b = s - d, s + d

        @pl.when((a >= 0) & has_up)
        def _():
            to_up(ow, a).wait_send()

        @pl.when((b < n_sp) & has_down)
        def _():
            to_down(ow, b).wait_send()


def spread_kernel(n_fs, n_tp, part, out, send, recv):
    s, f, t = place()
    others = [(lax.rem(f + d, n_fs), lax.rem(t + u, n_tp)) for d in range(n_fs) for u in range(n_tp)][1:]
    greet([(None, (s, g, u)) for g, u in others])
    copies = [
        rcopy(part.at[g, u], out.at[f, t], send.at[i], recv.at[f, t], (s, g, u)) for i, (g, u) in enumerate(others)
    ]
    for c in copies:
        c.start()
    out[f, t] = part[f, t]
    for c in copies:
        c.wait_send()
    for g, u in others:
        here = out.at[g, u]
        rcopy(here, here, send.at[0], recv.at[g, u], (s, g, u)).wait_recv()


def vmem(count):
    return [pl.BlockSpec(memory_space=pltpu.VMEM)] * count


def dma(*shape):
    return pltpu.SemaphoreType.DMA(shape) if shape else pltpu.SemaphoreType.DMA


def comm(kernel, outs, scratch, number, name):
    return pl.pallas_call(
        kernel,
        out_shape=[jax.ShapeDtypeStruct(a, b) for a, b in outs],
        out_specs=vmem(len(outs)),
        scratch_shapes=scratch,
        compiler_params=pltpu.CompilerParams(
            collective_id=number, has_side_effects=True, vmem_limit_bytes=60 * 1024 * 1024
        ),
        name=name,
    )


def local_recurrence(queries, input_gate, values, log_forget):
    tok_rows, head_count = (queries.shape[0], queries.shape[1])
    block_count = tok_rows // BLOCK
    q_blk, k_blk, v_blk, g_blk = (
        arr.reshape(block_count, BLOCK, head_count, HEAD_DIM)
        for arr in (queries, input_gate, values, log_forget)
    )
    within = jnp.cumsum(g_blk, axis=1)
    block_end = within[:, -1]
    q_up = q_blk * jnp.exp(within)
    k_down = k_blk * jnp.exp(-within)
    causal = jnp.tril(jnp.ones((BLOCK, BLOCK), jnp.bool_))
    scores = jnp.einsum("nthd,nshd->nhts", q_up, k_down, precision=HIGH)
    scores = jnp.where(causal, scores, 0.0)
    inner_out = jnp.einsum("nhts,nshe->nthe", scores, v_blk, precision=HIGH)
    updates = jnp.einsum(
        "nshd,nshe->nhde", k_blk * jnp.exp(block_end[:, None] - within), v_blk, precision=HIGH
    )
    decays = jnp.exp(block_end)
    state = jnp.zeros((head_count, HEAD_DIM, HEAD_DIM), F32)
    incoming = []
    for n in range(block_count):
        incoming.append(state)
        state = decays[n][:, :, None] * state + updates[n]
    offsets = jnp.cumsum(block_end, axis=0) - block_end
    total_log = jnp.sum(block_end, axis=0)
    return (inner_out, q_up, jnp.stack(incoming), jnp.exp(offsets), state, total_log)


def body(
    n_sp, n_fs, n_tp, tokens, norm_gain, w_query, forget_weight, w_input, w_outgate, w_pool, forget_gap,
    extra_decay, rec_gain, group_weight, pool_gain, recurrent_output_weight, w_out_pool,
):
    s, f, t = place()
    rows, half = tokens.shape[1:]
    width = w_query.shape[1]
    ch = width // n_fs
    n_w = 5
    wr = w_query.shape[0]
    stacked = jnp.stack(
        [w.reshape(wr, n_fs, ch) for w in (w_query, forget_weight, w_input, w_outgate, w_pool)], axis=2
    )
    wsrc = stacked.transpose(1, 0, 2, 3).reshape(n_fs, wr, n_w * ch)
    lanes = rows // 128
    extra = jnp.pad(extra_decay[0].T.reshape(n_fs, lanes, 128), ((0, 0), (0, 8 - lanes), (0, 0)))
    z, e_all = comm(
        functools.partial(project_kernel, n_sp, n_fs, n_tp),
        [((n_fs, rows, n_w * ch), BF), ((n_fs, 8, 128), F32)],
        [
            pltpu.VMEM((n_fs, rows, n_tp * half), BF), pltpu.VMEM((n_sp * n_fs * wr, n_w * ch), BF),
            dma(n_fs - 1), dma(n_fs), dma(n_fs), dma(n_fs), dma(n_fs - 1), dma(n_sp, n_fs),
            dma(n_sp, n_fs), dma(n_sp, n_fs), dma(n_fs - 1), dma(n_fs),
        ],
        1, "project",
    )(tokens[0], wsrc, extra, norm_gain[None])
    zf = z.astype(F32).transpose(1, 0, 2).reshape(rows, n_fs, n_w, ch)
    z_query, z_forget, z_input, z_outgate, z_pool = (zf[:, :, i] for i in range(n_w))
    gap = lax.dynamic_slice_in_dim(forget_gap, f * ch, ch, 0)
    gain = lax.dynamic_slice_in_dim(rec_gain, f * ch, ch, 0)
    decay_in = e_all[:, :lanes].reshape(n_fs, rows).T
    input_gate = gap * jax.nn.sigmoid(-z_forget)
    log_forget = jnp.log1p(-input_gate) + decay_in[:, :, None]
    inner_out, q_up, incoming, off, end_state, total_log = local_recurrence(
        jax.nn.silu(z_query), input_gate, z_input, log_forget
    )
    reach = 2**POOL_GROUPS
    tail = z[:, rows - reach :, (n_w - 1) * ch :]
    st, de, rim = comm(
        functools.partial(state_kernel, n_sp),
        [((n_sp - 1, n_fs, ch, ch), BF), ((n_sp - 1, n_fs, ch), F32), ((n_fs, reach, ch), BF)],
        [dma(n_sp - 1), dma(n_sp - 1), dma(n_sp - 1), dma(n_sp - 1), dma(), dma()],
        2, "state",
    )(end_state.astype(BF), jnp.exp(total_log), tail)
    total = jnp.zeros((n_fs, ch, ch), F32)
    for d in range(n_sp - 2, -1, -1):
        total = de[d][:, :, None] * total + st[d].astype(F32)
    entering = incoming + off[:, :, :, None] * total[None]
    recurrent = (inner_out + jnp.einsum("nthd,nhde->nthe", q_up, entering, precision=HIGH)).reshape(rows, n_fs, ch)
    square_sum = jnp.sum(recurrent * recurrent, axis=2)
    rec_act = (recurrent * gain * jax.nn.silu(z_outgate)).astype(BF).transpose(1, 0, 2).reshape(n_fs * rows, ch)
    sq = square_sum.T.reshape(n_fs * lanes, 128)

    zp = z[:, :, (n_w - 1) * ch :]
    running = jnp.concatenate([rim, zp], axis=1).astype(F32)
    group_dim = group_weight.shape[1]
    group = (t * width + f * ch) // group_dim
    window_total = None
    for level in range(POOL_GROUPS):
        stride = 2**level
        running = running[:, stride:] + running[:, :-stride]
        now = running[:, running.shape[1] - rows :]
        window_total = now if level == 0 else jnp.where(group == level, now, window_total)
    spot = s * rows + jnp.arange(rows, dtype=jnp.int32)
    counts = jnp.minimum(spot + 1, jnp.left_shift(jnp.int32(2), group)).astype(F32)
    pooled = (window_total / counts[None, :, None] - zp.astype(F32)).astype(BF).reshape(n_fs * rows, ch)

    groups_dev = w_out_pool.shape[0] // group_dim
    cw = w_out_pool.shape[1]
    local_map = lax.dynamic_slice_in_dim(group_weight, t * groups_dev, groups_dev, 0)
    scaled = (w_out_pool.astype(F32) * pool_gain[:, None]).astype(BF).reshape(groups_dev, group_dim, cw)
    folded = jnp.einsum("gcd,gdo->gco", local_map, scaled, preferred_element_type=F32).astype(BF)
    ow = jnp.concatenate(
        [recurrent_output_weight, folded.reshape(groups_dev * group_dim, cw)], axis=0
    ).reshape(-1, 128)
    n_half = n_sp // n_tp
    a_rec, a_pool, sq_all, ow_all = comm(
        functools.partial(mix_kernel, n_sp, n_fs, n_tp),
        [
            ((n_fs * rows, n_tp * width), BF), ((n_fs * rows, n_tp * width), BF),
            ((n_tp, n_fs) + sq.shape, F32), ((n_half, n_tp) + ow.shape, BF),
        ],
        [
            pltpu.VMEM((n_sp,) + ow.shape, BF),
            dma(n_fs - 1), dma(n_fs), dma(n_fs - 1), dma(n_fs), dma(n_tp, n_fs), dma(n_tp, n_fs),
            dma(n_fs), dma(n_fs), dma(n_fs), dma(n_fs),
            dma(n_sp), dma(n_sp), dma(n_sp), dma(n_sp), dma(n_sp),
        ],
        3, "mix",
    )(rec_act, pooled, sq, ow)
    ow_all = ow_all.reshape(n_half, n_tp, 2, width, cw)
    w_rec = ow_all[:, :, 0].transpose(1, 2, 0, 3).reshape(n_tp * width, n_half * cw)
    w_fold = ow_all[:, :, 1].transpose(1, 2, 0, 3).reshape(n_tp * width, n_half * cw)
    total_sq = jnp.sum(sq_all, axis=(0, 1)).reshape(n_fs * rows, 1)
    rec_scale = lax.rsqrt(total_sq / (n_tp * width) + EPS)
    mixed = (
        jnp.dot(a_rec, w_rec, preferred_element_type=F32) * rec_scale
        + jnp.dot(a_pool, w_fold, preferred_element_type=F32)
    ).astype(BF)
    mixed = mixed.reshape(n_fs, n_tp, rows // n_tp, n_half * cw)
    (final,) = comm(
        functools.partial(spread_kernel, n_fs, n_tp),
        [(mixed.shape, BF)],
        [dma(n_fs * n_tp), dma(n_fs, n_tp)],
        4, "spread",
    )(mixed)
    final = final.reshape(n_fs, n_tp, rows // n_tp, n_half, cw).transpose(2, 1, 3, 0, 4)
    return final.reshape(1, rows // n_tp, n_tp * n_half * n_fs * cw)


def solution(mesh):
    sizes = dict(mesh.shape)
    weight = P(("sp", "fs"), "tp")
    placed = (
        P("fs", "sp", "tp"), P(), weight, weight, weight, weight, weight, P("tp"),
        P("fs", "sp", "tp"), P("tp"), P(), P("tp"), P("tp", ("sp", "fs")), P("tp", ("sp", "fs")),
    )
    return jax.shard_map(
        functools.partial(body, sizes["sp"], sizes["fs"], sizes["tp"]),
        mesh=mesh, in_specs=placed, out_specs=P("fs", ("sp", "tp"), None), check_vma=False,
    )
```

time: 407 us -> 174 us (0.43)
  waiting for transfers between devices: 261 us -> 0 us
  Pallas kernels: 0 us -> 130 us
  blocking collectives: 81.7 us -> 0 us
  local copies, waits for them, and re-layouts: 9.23 us -> 25.4 us
  matrix products: 24 us -> 7.86 us
  between operations: 13.7 us -> 0.45 us
    all_gather x8 -> x0, waiting for transfers between devices: 251 us -> none  [the longest x1 59.8 us: body(): lax.all_gather(w_out_pool, ('sp', 'fs'), axis=1, tiled=True)]
    pallas_call x0 -> x4, Pallas kernels: none -> 130 us  [the longest x1 58.3 us: body(): comm(functools.partial(project_kernel, n_sp, n_fs, n_tp), [((n_fs, rows,...]
    all_gather x7 -> x0, blocking collectives: 75.9 us -> none  [the longest x2 29.3 us: carried_in(): lax.all_gather(a.astype(kind), axis)]
    dot_general x9 -> x4, matrix products: 20.8 us -> 5.52 us  [the longest x1 2.46 us: body(): jnp.dot(a_rec, w_rec, preferred_element_type=F32) * rec_scale]
    unnamed x36 -> x29, local copies, waits for them, and re-layouts: 0.52 us -> 8.83 us
    reduce_scatter x1 -> x0, waiting for transfers between devices: 7.94 us -> none  [body(): lax.psum_scatter((jnp.dot(recurrent_output, rec_columns, preferred_elemen...]
    psum x1 -> x0, blocking collectives: 5.82 us -> none  [body(): square_sum = lax.psum(jnp.sum(recurrent * recurrent, axis=1), 'tp')]
    another operation x8 -> x2, local copies, waits for them, and re-layouts: 5.83 us -> 0.54 us  [the longest x1 0.52 us: local_recurrence(): jnp.stack(incoming)]
  transfers between devices with their start and end apart: 10 -> 0, of which waited for: 7 -> 0; matrix products, arithmetic and copies ran while one was open for 11% -> 0% of each run, Pallas kernels for 0% -> 0%
where the time goes in v1:
time: 174 us
  Pallas kernels  130 us (75%)
  local copies, waits for them, and re-layouts  25.4 us (15%)
  other arithmetic  10.1 us (6%)
  matrix products  7.86 us (5%)
    pallas_call x1, Pallas kernels, body(): comm(functools.partial(project_kernel, n_sp, n_fs, n_tp), [((n_fs, rows,...  58.3 us
    pallas_call x1, Pallas kernels, body(): comm(functools.partial(mix_kernel, n_sp, n_fs, n_tp), [((n_fs * rows, n_t...  50.8 us
    pallas_call x1, Pallas kernels, body(): comm(functools.partial(state_kernel, n_sp), [((n_sp - 1, n_fs, ch, ch), B...  10.6 us
    pallas_call x1, Pallas kernels, body(): comm(functools.partial(spread_kernel, n_fs, n_tp), [(mixed.shape, BF)], [...  10.1 us
    unnamed x29, local copies, waits for them, and re-layouts  8.83 us

profile of v1, /device:TPU:1, one launch (start us, length us, event | category | flops | bytes accessed | tf_op | source)
XLA Modules:
  0.0 173.6 jit_solution(8981224630177448157)
XLA Ops:
  0.8 1.3 dynamic_slice.10
  4.0 1.0 copy.74
  5.0 1.0 copy.75
  6.1 1.0 copy.76
  7.1 1.0 copy.77
  8.1 1.0 copy.78
  9.2 1.0 multiply_convert_fusion.1
  11.3 1.1 copy.79.wsrc
  12.4 58.3 %project.1 = (bf16[4,256,640]{2,1,0:T(8,128)(2,1)}, f32[4,8,128]{2,1,0:T(8,128)}) custom-call(bf16[256,1024]{1,0:T(8,128)(2,1)} %bitcast.138, bf16[4,128,640]{2,1,0:T(8,128)(2,1)} %copy.79.wsrc, f32[4,8,128]{2,1,0:T(8,128)} %pad.4.extra, f32[1,2048]{1,0:T(1,128)} %bitcast.150), custom_call_target="tpu_custom_call" | custom-call | tf_op jit(solution)/shard_map/project/pallas_call | solution.py:385
  71.4 1.3 slice.121.edge
  73.9 1.6 copy.80
  76.3 1.5 copy-done.1
  83.6 10.6 %state.1 = (bf16[3,4,128,128]{3,2,1,0:T(8,128)(2,1)}, f32[3,4,128]{2,1,0:T(4,128)}, bf16[4,16,128]{2,1,0:T(8,128)(2,1)}) custom-call(bf16[4,128,128]{2,1,0:T(8,128)(2,1)} %fusion.35.state, f32[4,128]{1,0:T(4,128)} %exp.43.decay, bf16[4,16,128]{2,1,0:T(8,128)(2,1)} %slice.121.edge), custom_call_target="tpu_custom_call" | custom-call | tf_op jit(solution)/shard_map/state/pallas_call | solution.py:407
  94.9 1.3 add_bitcast_fusion
  96.2 1.3 multiply_reduce_fusion
  98.9 1.2 fusion.42
  101.2 2.0 %fusion.30 = bf16[4,256,128]{2,1,0:T(8,128)(2,1)} fusion(f32[4,271,128]{2,1,0:T(8,128)S(1)} %slice_add_fusion.2, f32[4,269,128]{2,1,0:T(8,128)S(1)} %slice_add_fusion.1, f32[4,265,128]{2,1,0:T(8,128)S(1)} %slice_add_fusion, f32[4,257,128]{2,1,0:T(8,128)S(1)} %get-tuple-element.31, f32[4,257,128]{2,1,0:T(8,128)S(1)} %get-tuple-element.30, ...), kind=kLoop, calls=%fused_computation.49 | loop fusion | flops 1048576 | bytes 3146755 | tf_op jit(solution)/shard_map/convert_element_type | solution.py:434
  103.2 50.8 %mix.1 = (bf16[1024,1024]{1,0:T(8,128)(2,1)}, bf16[1024,1024]{1,0:T(8,128)(2,1)}, f32[2,4,8,128]{3,2,1,0:T(8,128)}, bf16[2,2,1024,128]{3,2,1,0:T(8,128)(2,1)}) custom-call(bf16[1024,128]{1,0:T(8,128)(2,1)} %bitcast.135, bf16[1024,128]{1,0:T(8,128)(2,1)} %bitcast.134, f32[8,128]{1,0:T(8,128)} %reshape.125.sq, bf16[1024,128]{1,0:T(8,128)(2,1)} %pad_maximum_fusion.ow), custom_call_target="tpu_custom_call" | custom-call | tf_op jit(solution)/shard_map/mix/pallas_call | solution.py:445
  154.0 1.3 fusion.50
  156.5 2.5 %convolution_multiply_fusion = f32[1024,256]{1,0:T(8,128)S(1)} fusion(bf16[1024,1024]{1,0:T(8,128)(2,1)} %get-tuple-element.19, bf16[128,8,2,128]{3,2,1,0:T(2,128)(2,1)S(1)} %bitcast.141, f32[1024]{0:T(1024)S(1)} %rsqrt_bitcast_fusion), kind=kOutput, calls=%fused_computation.1 | convolution fusion | flops 537133056 | bytes 3674112 | tf_op jit(solution)/shard_map/dot_general | solution.py:465
  158.9 1.5 fusion
  160.5 10.1 %spread.1 = bf16[4,2,128,256]{3,2,1,0:T(8,128)(2,1)} custom-call(bf16[4,2,128,256]{3,2,1,0:T(8,128)(2,1)} %bitcast.133), custom_call_target="tpu_custom_call" | custom-call | tf_op jit(solution)/shard_map/spread/pallas_call | solution.py:469
  170.5 1.2 reshape.132
  172.4 1.2 reshape.133
  (69 shorter events, 16.9 us)
Async XLA Ops:
  0.0 10.2 %copy-start = (bf16[4,256,256]{2,1,0:T(8,128)(2,1)S(1)}, bf16[4,256,256]{2,1,0:T(8,128)(2,1)}, u32[]{:S(2)}) copy-start(bf16[4,256,256]{2,1,0:T(8,128)(2,1)} %param.24) | copy-start | bytes 1572868
  0.0 10.5 %copy-start.3 = (bf16[512,128]{1,0:T(8,128)(2,1)S(1)}, bf16[512,128]{1,0:T(8,128)(2,1)}, u32[]{:S(2)}) copy-start(bf16[512,128]{1,0:T(8,128)(2,1)} %param.26) | copy-start | bytes 393220
  76.2 1.5 copy-start.1
  82.3 13.9 %copy-start.7 = (f32[4]{0:T(128)S(1)}, f32[4]{0:T(128)}, u32[]{:S(2)}) copy-start(f32[4]{0:T(128)} %pad.9.clone) | copy-start | bytes 52
  94.2 4.1 %copy-start.5 = (bf16[4,16,128]{2,1,0:T(8,128)(2,1)S(1)}, bf16[4,16,128]{2,1,0:T(8,128)(2,1)}, u32[]{:S(2)}) copy-start(bf16[4,16,128]{2,1,0:T(8,128)(2,1)} %get-tuple-element.18) | copy-start | bytes 49156
  98.2 0.7 copy-start.6
  154.0 1.8 %copy-start.4 = (f32[2,4,8,128]{3,2,1,0:T(8,128)S(1)}, f32[2,4,8,128]{3,2,1,0:T(8,128)}, u32[]{:S(2)}) copy-start(f32[2,4,8,128]{3,2,1,0:T(8,128)} %get-tuple-element.21) | copy-start | bytes 98308
  156.5 2.5 %copy-start.2 = (bf16[1024,1024]{1,0:T(8,128)(2,1)S(1)}, bf16[1024,1024]{1,0:T(8,128)(2,1)}, u32[]{:S(2)}) copy-start(bf16[1024,1024]{1,0:T(8,128)(2,1)} %get-tuple-element.22) | copy-start | bytes 6291460

commit v2 on v1

--- a/solution.py
+++ b/solution.py
@@ -195,23 +195,31 @@
     pl.when(s > 0)(edge_copy.wait_recv)
 
 
+def square(f):
+    near = f + 1 - 2 * lax.rem(f, 2)
+    return near, lax.rem(f + 2, 4), lax.rem(near + 2, 4)
+
+
 def mix_kernel(
-    n_sp, n_fs, n_tp, rec, pool, sq, ow, a_rec, a_pool, sq_out, ow_out,
-    relay_buf, r_send, r_recv, p_send, p_recv, q_send, q_recv, dr_send, dr_recv, dp_send, dp_recv,
-    up_send, down_send, o_recv, od_send, od_recv,
+    n_sp, n_fs, n_tp, act, sq, ow, out,
+    acts, sq_all, ow_all, relay_buf, wbuf, part,
+    a_send, a_recv, f_send, d_send, d_recv, q_send, q_recv,
+    up_send, down_send, o_recv, od_send, od_recv, m_send, m_recv,
 ):
     s, f, t = place()
     n_half = n_sp // n_tp
+    rows = act.shape[1] // n_fs
+    half = rows // n_tp
+    width, cw = ow.shape[0] // 2, ow.shape[1]
     other = (s, f, 1 - t)
-    others = [lax.rem(f + d, n_fs) for d in range(1, n_fs)]
+    px, py, pd = square(f)
     up, down = (s + 1, f, t), (s - 1, f, t)
     has_up, has_down = s < n_sp - 1, s > 0
     greet(
-        [(None, other)] + [(None, (s, g, u)) for g in others for u in (t, 1 - t)] + [(has_up, up), (has_down, down)]
-    )
-
-    def cols(g, u):
-        return pl.ds(pl.multiple_of((u * n_fs + g) * HEAD_DIM, HEAD_DIM), HEAD_DIM)
+        [(None, other)]
+        + [(None, (s, g, u)) for g in (px, py, pd) for u in (t, 1 - t)]
+        + [(has_up, up), (has_down, down)]
+    )
 
     def to_up(src, a):
         return rcopy(src, relay_buf.at[a], up_send.at[a], o_recv.at[a], up)
@@ -220,42 +228,52 @@
         return rcopy(src, relay_buf.at[a], down_send.at[a], o_recv.at[a], down)
 
     def to_other(src, a):
-        return rcopy(src, ow_out.at[lax.rem(a, n_half), t], od_send.at[a], od_recv.at[a], other)
+        return rcopy(src, ow_all.at[lax.rem(a, n_half), t], od_send.at[a], od_recv.at[a], other)
 
     def keep(src, a):
         mine = a // n_half == t
 
         @pl.when(mine)
         def _():
-            ow_out[lax.rem(a, n_half), t] = src[...]
+            ow_all[lax.rem(a, n_half), t] = src[...]
 
         pl.when(jnp.logical_not(mine))(lambda: to_other(src, a).start())
 
+    sends = []
+
+    def send(c):
+        c.start()
+        sends.append(c)
+
+    for i, (p, order) in enumerate(((px, (0, 1)), (py, (1, 0)))):
+        for h in order:
+            send(rcopy(act.at[h], acts.at[t, f, h], a_send.at[i, h], a_recv.at[f, h], (s, p, t)))
     pl.when(has_up)(lambda: to_up(ow, s).start())
     pl.when(has_down)(lambda: to_down(ow, s).start())
-    sends = []
-    for d, g in enumerate(others):
-        sends.append(rcopy(pool, a_pool.at[:, cols(f, t)], p_send.at[d], p_recv.at[f], (s, g, t)))
-        sends.append(rcopy(rec, a_rec.at[:, cols(f, t)], r_send.at[d], r_recv.at[f], (s, g, t)))
+    for h in range(2):
+        send(rcopy(act.at[h], acts.at[t, f, h], d_send.at[f, h], d_recv.at[f, h], other))
+    for i, g in enumerate((px, py, pd)):
         for u in range(n_tp):
-            sends.append(rcopy(sq, sq_out.at[t, f], q_send.at[u, d], q_recv.at[t, f], (s, g, u)))
-    sends.append(rcopy(pool, a_pool.at[:, cols(f, t)], dp_send.at[f], dp_recv.at[f], other))
-    sends.append(rcopy(rec, a_rec.at[:, cols(f, t)], dr_send.at[f], dr_recv.at[f], other))
-    sends.append(rcopy(sq, sq_out.at[t, f], q_send.at[0, n_fs - 1], q_recv.at[t, f], other))
-    for c in sends:
-        c.start()
-    a_pool[:, cols(f, t)] = pool[...]
-    a_rec[:, cols(f, t)] = rec[...]
-    sq_out[t, f] = sq[...]
+            send(rcopy(sq, sq_all.at[t, f], q_send.at[i, u], q_recv.at[t, f], (s, g, u)))
+    send(rcopy(sq, sq_all.at[t, f], q_send.at[n_fs - 1, 0], q_recv.at[t, f], other))
+    acts[t, f] = act[...]
+    sq_all[t, f] = sq[...]
     keep(ow, s)
-    for d, g in enumerate(others):
-        for arr, rs, ds_, dr in ((a_pool, p_recv, dp_send, dp_recv), (a_rec, r_recv, dr_send, dr_recv)):
-            part = arr.at[:, cols(g, t)]
-            rcopy(part, part, ds_.at[g], rs.at[g], other).wait_recv()
-            c = rcopy(part, part, ds_.at[g], dr.at[g], other)
-            c.start()
-            sends.append(c)
-    for d in range(1, n_sp):
+
+    def landed(g, h):
+        here = acts.at[t, g, h]
+        rcopy(here, here, d_send.at[g, h], a_recv.at[g, h], other).wait_recv()
+        return here
+
+    def hand_on(g, h, here):
+        send(rcopy(here, here, d_send.at[g, h], d_recv.at[g, h], other))
+
+    for i, (g, h, onto) in enumerate(((px, 0, py), (py, 1, px))):
+        here = landed(g, h)
+        send(rcopy(here, here, f_send.at[i], a_recv.at[g, h], (s, onto, t)))
+        hand_on(g, h, here)
+
+    def step(d):
         a = s - d
 
         @pl.when(a >= 0)
@@ -270,50 +288,84 @@
             to_down(relay_buf.at[b], b).wait_recv()
             pl.when(has_down)(lambda: to_down(relay_buf.at[b], b).start())
             keep(relay_buf.at[b], b)
-    for g in [f] + others:
-        for arr, ds_, dr in ((a_pool, dp_send, dp_recv), (a_rec, dr_send, dr_recv)):
-            part = arr.at[:, cols(g, 1 - t)]
-            rcopy(part, part, ds_.at[g], dr.at[g], other).wait_recv()
-        for u in range(n_tp):
-            here = sq_out.at[u, g]
-            needed = rcopy(here, here, q_send.at[0, 0], q_recv.at[u, g], other)
-            pl.when(jnp.logical_or(g != f, u != t))(needed.wait_recv)
+
+    for d in range(1, n_sp):
+        step(d)
+    for g, h in ((px, 1), (py, 0), (pd, 0), (pd, 1)):
+        hand_on(g, h, landed(g, h))
     for i in range(n_half):
         a = t * n_half + i
-        here = ow_out.at[i, 1 - t]
+        here = ow_all.at[i, 1 - t]
         rcopy(here, here, od_send.at[a], od_recv.at[a], other).wait_recv()
+    for i in range(n_half):
+        for u in range(n_tp):
+            for k in range(2):
+                wbuf[k, u * width : (u + 1) * width, i * cw : (i + 1) * cw] = ow_all[i, u, k * width : (k + 1) * width, :]
+    for g in (px, py, pd):
+        for u in range(n_tp):
+            here = sq_all.at[u, g]
+            rcopy(here, here, q_send.at[0, 0], q_recv.at[u, g], other).wait_recv()
+    here = sq_all.at[1 - t, f]
+    rcopy(here, here, q_send.at[0, 0], q_recv.at[1 - t, f], other).wait_recv()
+    for g in (f, px, py, pd):
+        for h in range(2):
+            here = acts.at[1 - t, g, h]
+            rcopy(here, here, d_send.at[g, h], d_recv.at[g, h], other).wait_recv()
+
+    def piece(g, u):
+        return rcopy(part.at[g, u], out.at[f, t], m_send.at[g, u], m_recv.at[f, t], (s, g, u))
+
+    def spread(g):
+        for u in range(n_tp):
+            c = piece(g, u)
+            c.start()
+            sends.append(c)
+
+    last = None
+    for g in (pd, f, px, py):
+        here = pl.ds(pl.multiple_of(g * rows, rows), rows)
+        sums = sum(sq_all[u, i, g] for u in range(n_tp) for i in range(n_fs))
+        scale = lax.rsqrt(sums / (n_tp * width) + EPS).T
+        scale = jnp.concatenate([scale[:, i : i + 1] for i in range(rows // 128)], axis=0)
+        left = [
+            jnp.concatenate([acts[u, i, h, here, :] for u in range(n_tp) for i in range(n_fs)], axis=1)
+            for h in range(2)
+        ]
+        mixed = (
+            jnp.dot(left[0], wbuf[0], preferred_element_type=F32) * scale
+            + jnp.dot(left[1], wbuf[1], preferred_element_type=F32)
+        ).astype(BF)
+        for u in range(n_tp):
+            part[g, u] = mixed[u * half : (u + 1) * half]
+        if last is not None and last is not f:
+            spread(last)
+        if last is f:
+            c = piece(f, 1 - t)
+            c.start()
+            sends.append(c)
+        last = g
+    out[f, t] = part[f, t]
+    for i in range(n_half):
+        to_other(ow, (1 - t) * n_half + i).wait_send()
+    for d in range(n_sp):
+        a, b = s - d, s + d
+
+        @pl.when((a >= 0) & has_up)
+        def _():
+            to_up(ow, a).wait_send()
+
+        @pl.when((b < n_sp) & has_down)
+        def _():
+            to_down(ow, b).wait_send()
+    spread(last)
     for c in sends:
         c.wait_send()
-    for i in range(n_half):
-        a = (1 - t) * n_half + i
-        to_other(ow, a).wait_send()
-    for d in range(n_sp):
-        a, b = s - d, s + d
-
-        @pl.when((a >= 0) & has_up)
-        def _():
-            to_up(ow, a).wait_send()
-
-        @pl.when((b < n_sp) & has_down)
-        def _():
-            to_down(ow, b).wait_send()
-
-
-def spread_kernel(n_fs, n_tp, part, out, send, recv):
-    s, f, t = place()
-    others = [(lax.rem(f + d, n_fs), lax.rem(t + u, n_tp)) for d in range(n_fs) for u in range(n_tp)][1:]
-    greet([(None, (s, g, u)) for g, u in others])
-    copies = [
-        rcopy(part.at[g, u], out.at[f, t], send.at[i], recv.at[f, t], (s, g, u)) for i, (g, u) in enumerate(others)
-    ]
-    for c in copies:
-        c.start()
-    out[f, t] = part[f, t]
-    for c in copies:
-        c.wait_send()
-    for g, u in others:
-        here = out.at[g, u]
-        rcopy(here, here, send.at[0], recv.at[g, u], (s, g, u)).wait_recv()
+    for g in (px, py, pd):
+        for u in range(n_tp):
+            here = out.at[g, u]
+            rcopy(here, here, m_send.at[g, u], m_recv.at[g, u], other).wait_recv()
+    here = out.at[f, 1 - t]
+    rcopy(here, here, m_send.at[f, 1 - t], m_recv.at[f, 1 - t], other).wait_recv()
 
 
 def vmem(count):
@@ -417,7 +469,7 @@
     recurrent = (inner_out + jnp.einsum("nthd,nhde->nthe", q_up, entering, precision=HIGH)).reshape(rows, n_fs, ch)
     square_sum = jnp.sum(recurrent * recurrent, axis=2)
     rec_act = (recurrent * gain * jax.nn.silu(z_outgate)).astype(BF).transpose(1, 0, 2).reshape(n_fs * rows, ch)
-    sq = square_sum.T.reshape(n_fs * lanes, 128)
+    sq = jnp.pad(square_sum.T.reshape(n_fs, lanes, 128), ((0, 0), (0, 8 - lanes), (0, 0)))
 
     zp = z[:, :, (n_w - 1) * ch :]
     running = jnp.concatenate([rim, zp], axis=1).astype(F32)
@@ -438,40 +490,22 @@
     local_map = lax.dynamic_slice_in_dim(group_weight, t * groups_dev, groups_dev, 0)
     scaled = (w_out_pool.astype(F32) * pool_gain[:, None]).astype(BF).reshape(groups_dev, group_dim, cw)
     folded = jnp.einsum("gcd,gdo->gco", local_map, scaled, preferred_element_type=F32).astype(BF)
-    ow = jnp.concatenate(
-        [recurrent_output_weight, folded.reshape(groups_dev * group_dim, cw)], axis=0
-    ).reshape(-1, 128)
+    ow = jnp.concatenate([recurrent_output_weight, folded.reshape(groups_dev * group_dim, cw)], axis=0)
     n_half = n_sp // n_tp
-    a_rec, a_pool, sq_all, ow_all = comm(
+    act = jnp.stack([rec_act, pooled])
+    out_shape = (n_fs, n_tp, rows // n_tp, n_half * cw)
+    (final,) = comm(
         functools.partial(mix_kernel, n_sp, n_fs, n_tp),
+        [(out_shape, BF)],
         [
-            ((n_fs * rows, n_tp * width), BF), ((n_fs * rows, n_tp * width), BF),
-            ((n_tp, n_fs) + sq.shape, F32), ((n_half, n_tp) + ow.shape, BF),
-        ],
-        [
-            pltpu.VMEM((n_sp,) + ow.shape, BF),
-            dma(n_fs - 1), dma(n_fs), dma(n_fs - 1), dma(n_fs), dma(n_tp, n_fs), dma(n_tp, n_fs),
-            dma(n_fs), dma(n_fs), dma(n_fs), dma(n_fs),
-            dma(n_sp), dma(n_sp), dma(n_sp), dma(n_sp), dma(n_sp),
+            pltpu.VMEM((n_tp, n_fs) + act.shape, BF), pltpu.VMEM((n_tp, n_fs) + sq.shape, F32),
+            pltpu.VMEM((n_half, n_tp) + ow.shape, BF), pltpu.VMEM((n_sp,) + ow.shape, BF),
+            pltpu.VMEM((2, n_tp * width, n_half * cw), BF), pltpu.VMEM(out_shape, BF),
+            dma(2, 2), dma(n_fs, 2), dma(2), dma(n_fs, 2), dma(n_fs, 2), dma(n_fs, n_tp), dma(n_tp, n_fs),
+            dma(n_sp), dma(n_sp), dma(n_sp), dma(n_sp), dma(n_sp), dma(n_fs, n_tp), dma(n_fs, n_tp),
         ],
         3, "mix",
-    )(rec_act, pooled, sq, ow)
-    ow_all = ow_all.reshape(n_half, n_tp, 2, width, cw)
-    w_rec = ow_all[:, :, 0].transpose(1, 2, 0, 3).reshape(n_tp * width, n_half * cw)
-    w_fold = ow_all[:, :, 1].transpose(1, 2, 0, 3).reshape(n_tp * width, n_half * cw)
-    total_sq = jnp.sum(sq_all, axis=(0, 1)).reshape(n_fs * rows, 1)
-    rec_scale = lax.rsqrt(total_sq / (n_tp * width) + EPS)
-    mixed = (
-        jnp.dot(a_rec, w_rec, preferred_element_type=F32) * rec_scale
-        + jnp.dot(a_pool, w_fold, preferred_element_type=F32)
-    ).astype(BF)
-    mixed = mixed.reshape(n_fs, n_tp, rows // n_tp, n_half * cw)
-    (final,) = comm(
-        functools.partial(spread_kernel, n_fs, n_tp),
-        [(mixed.shape, BF)],
-        [dma(n_fs * n_tp), dma(n_fs, n_tp)],
-        4, "spread",
-    )(mixed)
+    )(act, sq, ow)
     final = final.reshape(n_fs, n_tp, rows // n_tp, n_half, cw).transpose(2, 1, 3, 0, 4)
     return final.reshape(1, rows // n_tp, n_tp * n_half * n_fs * cw)
 

time: 174 us -> 150 us (0.86)
  Pallas kernels: 130 us -> 112 us
  matrix products: 7.86 us -> 3.89 us
  local copies, waits for them, and re-layouts: 25.4 us -> 22 us
    pallas_call x2 -> x1, Pallas kernels: 60.9 us -> 42.8 us  [body(): comm(functools.partial(mix_kernel, n_sp, n_fs, n_tp), [(out_shape, BF)],...]
    dot_general x2 -> x0, matrix products: 3.97 us -> none  [the longest x1 2.46 us: body(): jnp.dot(a_rec, w_rec, preferred_element_type=F32) * rec_scale]
    unnamed x29 -> x21, local copies, waits for them, and re-layouts: 8.83 us -> 7.44 us
where the time goes in v2:
time: 150 us; the launch traced here: 149 us
  Pallas kernels  112 us (75%)
  local copies, waits for them, and re-layouts  22 us (15%)
  other arithmetic  11.1 us (7%)
  matrix products  3.89 us (3%)
    pallas_call x1, Pallas kernels, body(): comm(functools.partial(project_kernel, n_sp, n_fs, n_tp), [((n_fs, rows,...  58.2 us
    pallas_call x1, Pallas kernels, body(): comm(functools.partial(mix_kernel, n_sp, n_fs, n_tp), [(out_shape, BF)],...  42.8 us
    pallas_call x1, Pallas kernels, body(): comm(functools.partial(state_kernel, n_sp), [((n_sp - 1, n_fs, ch, ch), B...  10.6 us
    unnamed x21, local copies, waits for them, and re-layouts  7.44 us

profile of v2, /device:TPU:1, one launch (start us, length us, event | category | flops | bytes accessed | tf_op | source)
XLA Modules:
  0.0 149.1 jit_solution(2426711888646181128)
XLA Ops:
  0.8 1.3 dynamic_slice.10
  4.0 1.0 copy.70
  5.0 1.0 copy.71
  6.0 1.0 copy.72
  7.1 1.0 copy.73
  8.1 1.0 copy.74
  9.1 1.0 multiply_convert_fusion.1
  10.4 1.6 %pad_maximum_fusion.1.ow = bf16[1024,128]{1,0:T(8,128)(2,1)} fusion(bf16[512,128]{1,0:T(8,128)(2,1)S(1)} %bitcast.121, bf16[512,128]{1,0:T(8,128)(2,1)} %param.26), kind=kLoop, calls=%fused_computation.51 | loop fusion | flops 524288 | bytes 524288 | tf_op jit(solution)/shard_map/concatenate | solution.py:493
  12.2 1.1 copy.75.wsrc
  13.3 58.2 %project.1 = (bf16[4,256,640]{2,1,0:T(8,128)(2,1)}, f32[4,8,128]{2,1,0:T(8,128)}) custom-call(bf16[256,1024]{1,0:T(8,128)(2,1)} %bitcast.113, bf16[4,128,640]{2,1,0:T(8,128)(2,1)} %copy.75.wsrc, f32[4,8,128]{2,1,0:T(8,128)} %pad.7.extra, f32[1,2048]{1,0:T(1,128)} %bitcast.124), custom_call_target="tpu_custom_call" | custom-call | tf_op jit(solution)/shard_map/project/pallas_call | solution.py:437
  72.2 1.3 slice.115.edge
  73.7 1.0 slice.123
  74.7 1.6 %copy.76 = bf16[256,4,640]{0,2,1:T(8,128)(2,1)S(1)} copy(bf16[256,4,640]{2,0,1:T(8,128)(2,1)} %bitcast.104) | data formatting | bytes 2621440 | tf_op jit(solution)/shard_map/transpose | solution.py:447
  77.0 1.5 %copy-done.1 = f32[256,4,5,128]{0,3,2,1:T(8,128)} copy-done((f32[256,4,5,128]{0,3,2,1:T(8,128)}, f32[256,4,5,128]{0,3,2,1:T(8,128)S(1)}, u32[]{:S(2)}) %copy-start.1) | copy-done | bytes 2621464
  82.1 1.0 fusion.16
  83.1 1.0 fusion.30.state
  84.4 10.6 %state.1 = (bf16[3,4,128,128]{3,2,1,0:T(8,128)(2,1)}, f32[3,4,128]{2,1,0:T(4,128)}, bf16[4,16,128]{2,1,0:T(8,128)(2,1)}) custom-call(bf16[4,128,128]{2,1,0:T(8,128)(2,1)} %fusion.30.state, f32[4,128]{1,0:T(4,128)} %exp.43.decay, bf16[4,16,128]{2,1,0:T(8,128)(2,1)} %slice.115.edge), custom_call_target="tpu_custom_call" | custom-call | tf_op jit(solution)/shard_map/state/pallas_call | solution.py:459
  95.7 1.3 add_bitcast_fusion
  97.0 1.3 multiply_reduce_fusion
  99.4 1.2 fusion.37
  101.0 1.3 fusion.25
  103.2 42.8 %mix.1 = bf16[4,2,128,256]{3,2,1,0:T(8,128)(2,1)} custom-call(bf16[2,1024,128]{2,1,0:T(8,128)(2,1)} %pad_maximum_fusion.act, f32[4,8,128]{2,1,0:T(8,128)} %pad.8.sq, bf16[1024,128]{1,0:T(8,128)(2,1)} %pad_maximum_fusion.1.ow), custom_call_target="tpu_custom_call" | custom-call | tf_op jit(solution)/shard_map/mix/pallas_call | solution.py:497
  146.0 1.2 reshape.91
  147.9 1.2 reshape.92
  (57 shorter events, 11.9 us)
Async XLA Ops:
  0.0 10.2 %copy-start = (bf16[4,256,256]{2,1,0:T(8,128)(2,1)S(1)}, bf16[4,256,256]{2,1,0:T(8,128)(2,1)}, u32[]{:S(2)}) copy-start(bf16[4,256,256]{2,1,0:T(8,128)(2,1)} %param.24) | copy-start | bytes 1572868
  77.0 1.5 %copy-start.1 = (f32[256,4,5,128]{0,3,2,1:T(8,128)}, f32[256,4,5,128]{0,3,2,1:T(8,128)S(1)}, u32[]{:S(2)}) copy-start(f32[256,4,5,128]{0,3,2,1:T(8,128)S(1)} %reshape.85) | copy-start | bytes 7864324
  82.1 14.9 %copy-start.4 = (f32[4]{0:T(128)S(1)}, f32[4]{0:T(128)}, u32[]{:S(2)}) copy-start(f32[4]{0:T(128)} %pad.15.clone) | copy-start | bytes 52
  95.0 4.1 %copy-start.2 = (bf16[4,16,128]{2,1,0:T(8,128)(2,1)S(1)}, bf16[4,16,128]{2,1,0:T(8,128)(2,1)}, u32[]{:S(2)}) copy-start(bf16[4,16,128]{2,1,0:T(8,128)(2,1)} %get-tuple-element.14) | copy-start | bytes 49156
  98.3 1.1 copy-start.3

commit v3 on v2

--- a/solution.py
+++ b/solution.py
@@ -38,24 +38,39 @@
     pl.semaphore_wait(barrier, sum(1 if cond is None else jnp.where(cond, 1, 0) for cond, _ in devs))
 
 
+def square(f):
+    near = f + 1 - 2 * lax.rem(f, 2)
+    return near, lax.rem(f + 2, 4), lax.rem(near + 2, 4)
+
+
 def project_kernel(
-    n_sp, n_fs, n_tp, tok, wsrc, extra, gain, z_ref, e_ref,
-    xs, ws, xs_send, xs_recv, d_send, d_recv, w_send, w_recv, zr_send, zl_send, e_send, e_recv,
+    n_sp, n_fs, n_tp, tok, wq, wf, wi, wo, wp, extra, gain, gmap, pgain, wor, wop, z_ref, e_ref, ow_ref,
+    wsrc, xs, ws, acc, x_send, x_recv, f_send, d_send, d_recv, w_send, w_recv, zr_send, zl_send, e_send, e_recv,
 ):
     s, f, t = place()
     rows, half = tok.shape
-    wr = wsrc.shape[1]
+    part = rows // 2
+    mats = (wq, wf, wi, wo, wp)
+    wr, width = wq.shape
+    ch = width // n_fs
+    for i, w in enumerate(mats):
+        for g in range(n_fs):
+            wsrc[g, :, i * ch : (i + 1) * ch] = w[:, g * ch : (g + 1) * ch]
     other = (s, f, 1 - t)
-    others = [lax.rem(f + d, n_fs) for d in range(1, n_fs)]
+    px, py, pd = square(f)
+    order = (f, px, py, pd)
     up, down = (s + 1, f, t), (s - 1, f, t)
     has_up, has_down = s < n_sp - 1, s > 0
-    greet([(None, other)] + [(None, (s, g, t)) for g in others] + [(has_up, up), (has_down, down)])
+    greet([(None, other)] + [(None, (s, g, t)) for g in order[1:]] + [(has_up, up), (has_down, down)])
 
     def cols(c):
         return pl.ds(pl.multiple_of(c * half, half), half)
 
+    def span(a, b):
+        return pl.ds(pl.multiple_of((a * n_fs + b) * wr, wr), wr)
+
     def slot(a, b):
-        return ws.at[pl.ds(pl.multiple_of((a * n_fs + b) * wr, wr), wr), :]
+        return ws.at[span(a, b), :]
 
     def to_up(src, a, b):
         return rcopy(src, slot(a, b), zr_send.at[a, b], w_recv.at[a, b], up)
@@ -63,34 +78,55 @@
     def to_down(src, a, b):
         return rcopy(src, slot(a, b), zl_send.at[a, b], w_recv.at[a, b], down)
 
+    sends = []
+
+    def send(c):
+        c.start()
+        sends.append(c)
+
+    def x_slot(g, h, c):
+        return xs.at[g, h * part : (h + 1) * part, cols(c)]
+
     own = wsrc.at[f]
-    w_copies = [rcopy(wsrc.at[g], slot(s, f), w_send.at[d], w_recv.at[s, f], (s, g, t)) for d, g in enumerate(others)]
-    for c in w_copies:
-        c.start()
     pl.when(has_up)(lambda: to_up(own, s, f).start())
     pl.when(has_down)(lambda: to_down(own, s, f).start())
-    x_copies = [rcopy(tok, xs.at[f, :, cols(t)], xs_send.at[d], xs_recv.at[f], (s, g, t)) for d, g in enumerate(others)]
-    for c in x_copies:
-        c.start()
-    e_copies = [rcopy(extra.at[g], e_ref.at[f], e_send.at[d], e_recv.at[f], (s, g, t)) for d, g in enumerate(others)]
-    for c in e_copies:
-        c.start()
-    first = rcopy(tok, xs.at[f, :, cols(t)], d_send.at[f], d_recv.at[f], other)
-    first.start()
-    ws[pl.ds(pl.multiple_of((s * n_fs + f) * wr, wr), wr), :] = wsrc[f]
+    for i, g in enumerate((pd, px, py)):
+        send(rcopy(wsrc.at[g], slot(s, f), w_send.at[i], w_recv.at[s, f], (s, g, t)))
+    for i, (p, hs) in enumerate(((px, (0, 1)), (py, (1, 0)))):
+        for h in hs:
+            send(rcopy(tok.at[h * part : (h + 1) * part, :], x_slot(f, h, t), x_send.at[i, h], x_recv.at[f, h], (s, p, t)))
+    for h in range(2):
+        send(rcopy(tok.at[h * part : (h + 1) * part, :], x_slot(f, h, t), d_send.at[f, h], d_recv.at[f, h], other))
+    for i, g in enumerate(order[1:]):
+        send(rcopy(extra.at[g], e_ref.at[f], e_send.at[i], e_recv.at[f], (s, g, t)))
+    ws[span(s, f), :] = wsrc[f]
     xs[f, :, cols(t)] = tok[...]
     e_ref[f] = extra[f]
-
-    for g in others:
+    ow_ref[0:width, :] = wor[...]
+    gd = gmap.shape[1]
+    for i in range(width // gd):
+        at = slice(i * gd, (i + 1) * gd)
+        scaled = (gmap[t * (width // gd) + i].astype(F32) * pgain[:, at]).astype(BF)
+        folded = jnp.dot(scaled, wop[at, :], preferred_element_type=F32)
+        ow_ref[width + i * gd : width + (i + 1) * gd, :] = folded.astype(BF)
+
+    for g in order[1:]:
         to_up(slot(s, g), s, g).wait_recv()
         pl.when(has_up)(lambda: to_up(slot(s, g), s, g).start())
         pl.when(has_down)(lambda: to_down(slot(s, g), s, g).start())
 
-    def swap(g):
-        part = xs.at[g, :, cols(t)]
-        return rcopy(part, part, d_send.at[g], d_recv.at[g], other)
-
-    order = [f] + others
+    def landed(g, h):
+        here = x_slot(g, h, t)
+        rcopy(here, here, d_send.at[g, h], x_recv.at[g, h], other).wait_recv()
+        return here
+
+    def hand_on(g, h, here):
+        send(rcopy(here, here, d_send.at[g, h], d_recv.at[g, h], other))
+
+    for i, (g, h, onto) in enumerate(((px, 0, py), (py, 1, px))):
+        here = landed(g, h)
+        send(rcopy(here, here, f_send.at[i], x_recv.at[g, h], (s, onto, t)))
+        hand_on(g, h, here)
 
     def relay(d):
         for g in order:
@@ -107,37 +143,68 @@
                 to_down(slot(b, g), b, g).wait_recv()
                 pl.when(has_down)(lambda: to_down(slot(b, g), b, g).start())
 
-    def norm(g):
-        theirs = xs.at[g, :, cols(1 - t)]
-        rcopy(theirs, theirs, d_send.at[g], d_recv.at[g], other).wait_recv()
-        step = 32
-        for i in range(rows // step):
-            feats = xs[g, pl.ds(i * step, step), :].astype(F32)
-            scale = lax.rsqrt(jnp.mean(feats * feats, axis=-1, keepdims=True) + EPS)
-            xs[g, pl.ds(i * step, step), :] = (feats * scale * gain[...]).astype(BF)
+    def add(a):
+        k = pl.ds(pl.multiple_of(a * n_fs * wr, n_fs * wr), n_fs * wr)
+
+        def each(i, _):
+            acc[i] += jnp.dot(xs[i, :, k], ws[k, :], preferred_element_type=F32)
+            return 0
+
+        lax.fori_loop(0, n_fs, each, 0)
+
+    def multiply(d):
+        pl.when(s - d >= 0)(lambda: add(s - d))
+        pl.when(s + d < n_sp)(lambda: add(s + d))
 
     relay(1)
-    for i, g in enumerate(others):
-        part = xs.at[g, :, cols(t)]
-        rcopy(part, part, xs_send.at[i], xs_recv.at[g], other).wait_recv()
-        swap(g).start()
-    for d in range(2, n_sp):
+    for g, h in ((px, 1), (py, 0), (pd, 0), (pd, 1)):
+        hand_on(g, h, landed(g, h))
+    for d in range(2, n_sp - 1):
         relay(d)
-    for c in w_copies + x_copies + e_copies:
+    for g in order:
+        for h in range(2):
+            here = x_slot(g, h, 1 - t)
+            rcopy(here, here, d_send.at[g, h], d_recv.at[g, h], other).wait_recv()
+    for g in order[1:]:
+        rcopy(extra.at[f], e_ref.at[g], e_send.at[0], e_recv.at[g], other).wait_recv()
+    for c in sends:
         c.wait_send()
-    for g in others:
-        rcopy(extra.at[f], e_ref.at[g], e_send.at[0], e_recv.at[g], other).wait_recv()
-    first.wait_send()
-    for g in others:
-        swap(g).wait_send()
-    for g in order:
-        norm(g)
-
-    def each(i, _):
-        z_ref[i] = jnp.dot(xs[i], ws[...], preferred_element_type=F32).astype(BF)
+
+    def norm(j, _):
+        tile = 16
+        per = rows // tile
+        at = (j // per, pl.ds(pl.multiple_of(lax.rem(j, per) * tile, tile), tile))
+        feats = xs[at[0], at[1], :].astype(F32)
+        scale = lax.rsqrt(jnp.mean(feats * feats, axis=-1, keepdims=True) + EPS)
+        xs[at[0], at[1], :] = (feats * scale * gain[...]).astype(BF)
         return 0
 
-    lax.fori_loop(0, n_fs, each, 0)
+    lax.fori_loop(0, n_fs * rows // 16, norm, 0, unroll=2)
+
+    if n_fs * wr % 128 == 0:
+        own_k = pl.ds(pl.multiple_of(s * n_fs * wr, n_fs * wr), n_fs * wr)
+
+        def begin(i, _):
+            acc[i] = jnp.dot(xs[i, :, own_k], ws[own_k, :], preferred_element_type=F32)
+            return 0
+
+        lax.fori_loop(0, n_fs, begin, 0)
+        for d in range(1, n_sp - 1):
+            multiply(d)
+        relay(n_sp - 1)
+        multiply(n_sp - 1)
+
+        def finish(i, _):
+            z_ref[i] = acc[i].astype(BF)
+            return 0
+    else:
+        relay(n_sp - 1)
+
+        def finish(i, _):
+            z_ref[i] = jnp.dot(xs[i], ws[...], preferred_element_type=F32).astype(BF)
+            return 0
+
+    lax.fori_loop(0, n_fs, finish, 0)
 
     for d in range(n_sp):
         for g in order:
@@ -193,11 +260,6 @@
                 c.wait_send()
     pl.when(s < n_sp - 1)(edge_copy.wait_send)
     pl.when(s > 0)(edge_copy.wait_recv)
-
-
-def square(f):
-    near = f + 1 - 2 * lax.rem(f, 2)
-    return near, lax.rem(f + 2, 4), lax.rem(near + 2, 4)
 
 
 def mix_kernel(
@@ -428,22 +490,23 @@
     ch = width // n_fs
     n_w = 5
     wr = w_query.shape[0]
-    stacked = jnp.stack(
-        [w.reshape(wr, n_fs, ch) for w in (w_query, forget_weight, w_input, w_outgate, w_pool)], axis=2
-    )
-    wsrc = stacked.transpose(1, 0, 2, 3).reshape(n_fs, wr, n_w * ch)
     lanes = rows // 128
     extra = jnp.pad(extra_decay[0].T.reshape(n_fs, lanes, 128), ((0, 0), (0, 8 - lanes), (0, 0)))
-    z, e_all = comm(
+    cw = w_out_pool.shape[1]
+    z, e_all, ow = comm(
         functools.partial(project_kernel, n_sp, n_fs, n_tp),
-        [((n_fs, rows, n_w * ch), BF), ((n_fs, 8, 128), F32)],
+        [((n_fs, rows, n_w * ch), BF), ((n_fs, 8, 128), F32), ((2 * width, cw), BF)],
         [
-            pltpu.VMEM((n_fs, rows, n_tp * half), BF), pltpu.VMEM((n_sp * n_fs * wr, n_w * ch), BF),
-            dma(n_fs - 1), dma(n_fs), dma(n_fs), dma(n_fs), dma(n_fs - 1), dma(n_sp, n_fs),
+            pltpu.VMEM((n_fs, wr, n_w * ch), BF), pltpu.VMEM((n_fs, rows, n_tp * half), BF),
+            pltpu.VMEM((n_sp * n_fs * wr, n_w * ch), BF), pltpu.VMEM((n_fs, rows, n_w * ch), F32),
+            dma(2, 2), dma(n_fs, 2), dma(2), dma(n_fs, 2), dma(n_fs, 2), dma(n_fs - 1), dma(n_sp, n_fs),
             dma(n_sp, n_fs), dma(n_sp, n_fs), dma(n_fs - 1), dma(n_fs),
         ],
         1, "project",
-    )(tokens[0], wsrc, extra, norm_gain[None])
+    )(
+        tokens[0], w_query, forget_weight, w_input, w_outgate, w_pool, extra, norm_gain[None],
+        group_weight, pool_gain[None], recurrent_output_weight, w_out_pool,
+    )
     zf = z.astype(F32).transpose(1, 0, 2).reshape(rows, n_fs, n_w, ch)
     z_query, z_forget, z_input, z_outgate, z_pool = (zf[:, :, i] for i in range(n_w))
     gap = lax.dynamic_slice_in_dim(forget_gap, f * ch, ch, 0)
@@ -485,12 +548,6 @@
     counts = jnp.minimum(spot + 1, jnp.left_shift(jnp.int32(2), group)).astype(F32)
     pooled = (window_total / counts[None, :, None] - zp.astype(F32)).astype(BF).reshape(n_fs * rows, ch)
 
-    groups_dev = w_out_pool.shape[0] // group_dim
-    cw = w_out_pool.shape[1]
-    local_map = lax.dynamic_slice_in_dim(group_weight, t * groups_dev, groups_dev, 0)
-    scaled = (w_out_pool.astype(F32) * pool_gain[:, None]).astype(BF).reshape(groups_dev, group_dim, cw)
-    folded = jnp.einsum("gcd,gdo->gco", local_map, scaled, preferred_element_type=F32).astype(BF)
-    ow = jnp.concatenate([recurrent_output_weight, folded.reshape(groups_dev * group_dim, cw)], axis=0)
     n_half = n_sp // n_tp
     act = jnp.stack([rec_act, pooled])
     out_shape = (n_fs, n_tp, rows // n_tp, n_half * cw)

time: 150 us -> 135 us (0.900)
  local copies, waits for them, and re-layouts: 22 us -> 14.5 us
  Pallas kernels: 112 us -> 107 us
  other arithmetic: 11.1 us -> 8.47 us
    unnamed x21 -> x6, local copies, waits for them, and re-layouts: 7.44 us -> 2.23 us
    pallas_call x1, Pallas kernels: 58.2 us -> 54.3 us  [body(): comm(functools.partial(project_kernel, n_sp, n_fs, n_tp), [((n_fs, rows,...]
    concatenate x1 -> x0, other arithmetic: 1.62 us -> none  [body(): jnp.concatenate([recurrent_output_weight, folded.reshape(groups_dev * gro...]
    pallas_call x1, Pallas kernels: 10.6 us -> 9.07 us  [body(): comm(functools.partial(state_kernel, n_sp), [((n_sp - 1, n_fs, ch, ch), B...]
where the time goes in v3:
time: 135 us; the launch traced here: 134 us
  Pallas kernels  107 us (79%)
  local copies, waits for them, and re-layouts  14.5 us (11%)
  other arithmetic  8.47 us (6%)
  matrix products  3.67 us (3%)
    pallas_call x1, Pallas kernels, body(): comm(functools.partial(project_kernel, n_sp, n_fs, n_tp), [((n_fs, rows,...  54.3 us
    pallas_call x1, Pallas kernels, body(): comm(functools.partial(mix_kernel, n_sp, n_fs, n_tp), [(out_shape, BF)],...  43.8 us
    pallas_call x1, Pallas kernels, body(): comm(functools.partial(state_kernel, n_sp), [((n_sp - 1, n_fs, ch, ch), B...  9.07 us

profile of v3, /device:TPU:1, one launch (start us, length us, event | category | flops | bytes accessed | tf_op | source)
XLA Modules:
  0.0 134.1 jit_solution(16198376801026501513)
XLA Ops:
  0.0 0.8 dynamic_slice.6
  0.8 0.8 dynamic_slice.7
  1.5 0.7 reshape.72
  2.8 54.3 %project.1 = (bf16[4,256,640]{2,1,0:T(8,128)(2,1)}, f32[4,8,128]{2,1,0:T(8,128)}, bf16[1024,128]{1,0:T(8,128)(2,1)}) custom-call(bf16[256,1024]{1,0:T(8,128)(2,1)} %bitcast.102, bf16[128,512]{1,0:T(8,128)(2,1)} %wq.1, bf16[128,512]{1,0:T(8,128)(2,1)} %wf.1, bf16[128,512]{1,0:T(8,128)(2,1)} %wi.1, bf16[128,512]{1,0:T(8,128)(2,1)} %wo.1, bf16[128,512]{1,0:T(8,128)(2,1)} %wp.1, ...), custom_call_target="tpu_custom_call" | custom-call | tf_op jit(solution)/shard_map/project/pallas_call | solution.py:496
  57.1 0.7 slice_bitcast_fusion.3
  57.9 1.3 slice.115.edge
  59.3 1.0 slice.123
  60.3 1.6 %copy.53 = bf16[256,4,640]{0,2,1:T(8,128)(2,1)S(1)} copy(bf16[256,4,640]{2,0,1:T(8,128)(2,1)} %bitcast.94) | data formatting | bytes 2621440 | tf_op jit(solution)/shard_map/transpose | solution.py:510
  62.7 1.5 %copy-done = f32[256,4,5,128]{0,3,2,1:T(8,128)} copy-done((f32[256,4,5,128]{0,3,2,1:T(8,128)}, f32[256,4,5,128]{0,3,2,1:T(8,128)S(1)}, u32[]{:S(2)}) %copy-start) | copy-done | bytes 2621464
  65.7 0.7 exponential_multiply_fusion.1
  66.4 1.0 convolution_select_fusion
  67.7 1.0 fusion.16
  68.7 1.0 fusion.30.state
  70.0 9.1 %state.1 = (bf16[3,4,128,128]{3,2,1,0:T(8,128)(2,1)}, f32[3,4,128]{2,1,0:T(4,128)}, bf16[4,16,128]{2,1,0:T(8,128)(2,1)}) custom-call(bf16[4,128,128]{2,1,0:T(8,128)(2,1)} %fusion.30.state, f32[4,128]{1,0:T(4,128)} %exp.43.decay, bf16[4,16,128]{2,1,0:T(8,128)(2,1)} %slice.115.edge), custom_call_target="tpu_custom_call" | custom-call | tf_op jit(solution)/shard_map/state/pallas_call | solution.py:522
  79.1 0.7 slice_bitcast_fusion.8
  79.8 1.3 add_bitcast_fusion
  81.1 1.3 multiply_reduce_fusion
  83.5 1.2 fusion.36
  85.1 1.3 fusion.25
  86.4 0.8 pad_maximum_fusion.act
  87.3 43.8 %mix.1 = bf16[4,2,128,256]{3,2,1,0:T(8,128)(2,1)} custom-call(bf16[2,1024,128]{2,1,0:T(8,128)(2,1)} %pad_maximum_fusion.act, f32[4,8,128]{2,1,0:T(8,128)} %pad.8.sq, bf16[1024,128]{1,0:T(8,128)(2,1)} %get-tuple-element.16.ow), custom_call_target="tpu_custom_call" | custom-call | tf_op jit(solution)/shard_map/mix/pallas_call | solution.py:554
  131.0 1.2 reshape.78
  132.2 0.7 copy.69
  132.9 1.2 reshape.79
  (37 shorter events, 5.0 us)
Async XLA Ops:
  62.7 1.5 %copy-start = (f32[256,4,5,128]{0,3,2,1:T(8,128)}, f32[256,4,5,128]{0,3,2,1:T(8,128)S(1)}, u32[]{:S(2)}) copy-start(f32[256,4,5,128]{0,3,2,1:T(8,128)S(1)} %reshape.74) | copy-start | bytes 7864324
  79.1 4.1 %copy-start.1 = (bf16[4,16,128]{2,1,0:T(8,128)(2,1)S(1)}, bf16[4,16,128]{2,1,0:T(8,128)(2,1)}, u32[]{:S(2)}) copy-start(bf16[4,16,128]{2,1,0:T(8,128)(2,1)} %get-tuple-element.15) | copy-start | bytes 49156

commit v4 on v3

--- a/solution.py
+++ b/solution.py
@@ -220,22 +220,66 @@
                 to_down(slot(b, g), b, g).wait_send()
 
 
-def state_kernel(n_sp, state, decay, edge, st_out, de_out, ed_out, s_send, s_recv, c_send, c_recv, g_send, g_recv):
+def dot(a, b, dims):
+    return lax.dot_general(a, b, (dims, ((), ())), precision=HIGH, preferred_element_type=F32)
+
+
+def state_kernel(
+    n_sp, group_dim, z, e_all, gap, rec_gain, act, sq_out,
+    local, qd, own_st, own_de, st_in, de_in, rim, s_send, s_recv, c_send, c_recv, g_send, g_recv,
+):
     s, f, t = place()
+    n_fs, rows, _ = z.shape
+    ch = HEAD_DIM
+    reach = rim.shape[1]
     devs = []
     for d in range(1, n_sp):
         devs.append((s + d < n_sp, (s + d, f, t)))
         devs.append((s - d >= 0, (s - d, f, t)))
     greet(devs)
-    nxt = (s + 1, f, t)
-    edge_copy = rcopy(edge, ed_out, g_send, g_recv, nxt)
-    pl.when(s < n_sp - 1)(edge_copy.start)
+    edge = rcopy(z.at[:, rows - reach :, 4 * ch :], rim, g_send, g_recv, (s + 1, f, t))
+    pl.when(s < n_sp - 1)(edge.start)
+    mine = pl.ds(pl.multiple_of(f * ch, ch), ch)
+    gap_f = gap[:, mine]
+    gain_f = rec_gain[:, mine]
+    at = lax.broadcasted_iota(jnp.int32, (BLOCK, BLOCK), 0)
+    causal = at >= lax.broadcasted_iota(jnp.int32, (BLOCK, BLOCK), 1)
+    lower = causal.astype(F32)
+
+    def one(g, _):
+        state = jnp.zeros((ch, ch), F32)
+        so_far = jnp.zeros((1, ch), F32)
+        e_cols = e_all[g].T
+        for n in range(rows // BLOCK):
+            here = slice(n * BLOCK, (n + 1) * BLOCK)
+            q, fo, v = (z[g, here, i * ch : (i + 1) * ch].astype(F32) for i in range(3))
+            q = jax.nn.silu(q)
+            k = gap_f * jax.nn.sigmoid(-fo)
+            lo = n * BLOCK % 128
+            lane = n * BLOCK // 128
+            logs = jnp.log1p(-k) + e_cols[lo : lo + BLOCK, lane : lane + 1]
+            within = dot(lower, logs, ((1,), (0,)))
+            end = within[BLOCK - 1 :]
+            q_up = q * jnp.exp(within)
+            scores = jnp.where(causal, dot(q_up, k * jnp.exp(-within), ((1,), (1,))), 0.0)
+            out = dot(scores, v, ((1,), (0,)))
+            if n:
+                out = out + dot(q_up, state, ((1,), (1,)))
+            local[g, here, :] = out
+            qd[g, here, :] = q_up * jnp.exp(so_far)
+            state = state * jnp.exp(end) + dot(v.T, k * jnp.exp(end - within), ((1,), (0,)))
+            so_far = so_far + end
+        own_st[g] = state.astype(BF)
+        own_de[g] = jnp.broadcast_to(jnp.exp(so_far), (8, ch))
+        return 0
+
+    lax.fori_loop(0, n_fs, one, 0)
 
     def pair(d):
         dev = (s + d, f, t)
         return (
-            rcopy(state, st_out.at[d - 1], s_send.at[d - 1], s_recv.at[d - 1], dev),
-            rcopy(decay, de_out.at[d - 1], c_send.at[d - 1], c_recv.at[d - 1], dev),
+            rcopy(own_st, st_in.at[d - 1], s_send.at[d - 1], s_recv.at[d - 1], dev),
+            rcopy(own_de, de_in.at[d - 1], c_send.at[d - 1], c_recv.at[d - 1], dev),
         )
 
     for d in range(1, n_sp):
@@ -243,23 +287,57 @@
         def _():
             for c in pair(d):
                 c.start()
-    pl.when(s == 0)(lambda: ed_out.__setitem__(Ellipsis, jnp.zeros(ed_out.shape, ed_out.dtype)))
-    for d in range(1, n_sp):
+
         @pl.when(s - d < 0)
         def _():
-            st_out[d - 1] = jnp.zeros(st_out.shape[1:], st_out.dtype)
-            de_out[d - 1] = jnp.ones(de_out.shape[1:], de_out.dtype)
+            st_in[d - 1] = jnp.zeros(st_in.shape[1:], st_in.dtype)
+            de_in[d - 1] = jnp.ones(de_in.shape[1:], de_in.dtype)
+    pl.when(s == 0)(lambda: rim.__setitem__(Ellipsis, jnp.zeros(rim.shape, rim.dtype)))
+    pl.when(s > 0)(edge.wait_recv)
+    group = (t * n_fs * ch + f * ch) // group_dim
+    spot = s * rows + lax.broadcasted_iota(jnp.int32, (rows, ch), 0)
+    window = 2
+    for level in range(1, POOL_GROUPS):
+        window = jnp.where(group == level, 2 ** (level + 1), window)
+    counts = jnp.minimum(spot + 1, window).astype(F32)
+    for g in range(n_fs):
+        zp = z[g, :, 4 * ch :].astype(F32)
+        running = jnp.concatenate([rim[g].astype(F32), zp], axis=0)
+        total = None
+        for level in range(POOL_GROUPS):
+            stride = 2**level
+            running = running[stride:] + running[:-stride]
+            now = running[running.shape[0] - rows :]
+            total = now if level == 0 else jnp.where(group == level, now, total)
+        act[1, g * rows : (g + 1) * rows, :] = (total / counts - zp).astype(BF)
     for d in range(1, n_sp):
         @pl.when(s - d >= 0)
         def _():
             for c in pair(d):
                 c.wait_recv()
+
+    ones = jnp.ones((8, ch), F32)
+
+    def finish(g, _):
+        total = jnp.zeros((ch, ch), F32)
+        for d in range(n_sp - 2, -1, -1):
+            total = de_in[d, g, 0:1, :] * total + st_in[d, g].astype(F32)
+        rec = local[g] + dot(qd[g], total, ((1,), (1,)))
+        sums = dot(ones, rec * rec, ((1,), (1,)))
+        for i in range(rows // 128):
+            sq_out[g, i : i + 1, :] = sums[0:1, i * 128 : (i + 1) * 128]
+        gate = jax.nn.silu(z[g, :, 3 * ch : 4 * ch].astype(F32))
+        act[0, pl.ds(pl.multiple_of(g * rows, rows), rows), :] = (rec * gain_f * gate).astype(BF)
+        return 0
+
+    sq_out[...] = jnp.zeros(sq_out.shape, F32)
+    lax.fori_loop(0, n_fs, finish, 0)
+    for d in range(1, n_sp):
         @pl.when(s + d < n_sp)
         def _():
             for c in pair(d):
                 c.wait_send()
-    pl.when(s < n_sp - 1)(edge_copy.wait_send)
-    pl.when(s > 0)(edge_copy.wait_recv)
+    pl.when(s < n_sp - 1)(edge.wait_send)
 
 
 def mix_kernel(
@@ -451,35 +529,6 @@
     )
 
 
-def local_recurrence(queries, input_gate, values, log_forget):
-    tok_rows, head_count = (queries.shape[0], queries.shape[1])
-    block_count = tok_rows // BLOCK
-    q_blk, k_blk, v_blk, g_blk = (
-        arr.reshape(block_count, BLOCK, head_count, HEAD_DIM)
-        for arr in (queries, input_gate, values, log_forget)
-    )
-    within = jnp.cumsum(g_blk, axis=1)
-    block_end = within[:, -1]
-    q_up = q_blk * jnp.exp(within)
-    k_down = k_blk * jnp.exp(-within)
-    causal = jnp.tril(jnp.ones((BLOCK, BLOCK), jnp.bool_))
-    scores = jnp.einsum("nthd,nshd->nhts", q_up, k_down, precision=HIGH)
-    scores = jnp.where(causal, scores, 0.0)
-    inner_out = jnp.einsum("nhts,nshe->nthe", scores, v_blk, precision=HIGH)
-    updates = jnp.einsum(
-        "nshd,nshe->nhde", k_blk * jnp.exp(block_end[:, None] - within), v_blk, precision=HIGH
-    )
-    decays = jnp.exp(block_end)
-    state = jnp.zeros((head_count, HEAD_DIM, HEAD_DIM), F32)
-    incoming = []
-    for n in range(block_count):
-        incoming.append(state)
-        state = decays[n][:, :, None] * state + updates[n]
-    offsets = jnp.cumsum(block_end, axis=0) - block_end
-    total_log = jnp.sum(block_end, axis=0)
-    return (inner_out, q_up, jnp.stack(incoming), jnp.exp(offsets), state, total_log)
-
-
 def body(
     n_sp, n_fs, n_tp, tokens, norm_gain, w_query, forget_weight, w_input, w_outgate, w_pool, forget_gap,
     extra_decay, rec_gain, group_weight, pool_gain, recurrent_output_weight, w_out_pool,
@@ -507,49 +556,19 @@
         tokens[0], w_query, forget_weight, w_input, w_outgate, w_pool, extra, norm_gain[None],
         group_weight, pool_gain[None], recurrent_output_weight, w_out_pool,
     )
-    zf = z.astype(F32).transpose(1, 0, 2).reshape(rows, n_fs, n_w, ch)
-    z_query, z_forget, z_input, z_outgate, z_pool = (zf[:, :, i] for i in range(n_w))
-    gap = lax.dynamic_slice_in_dim(forget_gap, f * ch, ch, 0)
-    gain = lax.dynamic_slice_in_dim(rec_gain, f * ch, ch, 0)
-    decay_in = e_all[:, :lanes].reshape(n_fs, rows).T
-    input_gate = gap * jax.nn.sigmoid(-z_forget)
-    log_forget = jnp.log1p(-input_gate) + decay_in[:, :, None]
-    inner_out, q_up, incoming, off, end_state, total_log = local_recurrence(
-        jax.nn.silu(z_query), input_gate, z_input, log_forget
-    )
-    reach = 2**POOL_GROUPS
-    tail = z[:, rows - reach :, (n_w - 1) * ch :]
-    st, de, rim = comm(
-        functools.partial(state_kernel, n_sp),
-        [((n_sp - 1, n_fs, ch, ch), BF), ((n_sp - 1, n_fs, ch), F32), ((n_fs, reach, ch), BF)],
-        [dma(n_sp - 1), dma(n_sp - 1), dma(n_sp - 1), dma(n_sp - 1), dma(), dma()],
+    n_half = n_sp // n_tp
+    act, sq = comm(
+        functools.partial(state_kernel, n_sp, group_weight.shape[1]),
+        [((2, n_fs * rows, ch), BF), ((n_fs, 8, 128), F32)],
+        [
+            pltpu.VMEM((n_fs, rows, ch), F32), pltpu.VMEM((n_fs, rows, ch), F32),
+            pltpu.VMEM((n_fs, ch, ch), BF), pltpu.VMEM((n_fs, 8, ch), F32),
+            pltpu.VMEM((n_sp - 1, n_fs, ch, ch), BF), pltpu.VMEM((n_sp - 1, n_fs, 8, ch), F32),
+            pltpu.VMEM((n_fs, 2**POOL_GROUPS, ch), BF),
+            dma(n_sp - 1), dma(n_sp - 1), dma(n_sp - 1), dma(n_sp - 1), dma(), dma(),
+        ],
         2, "state",
-    )(end_state.astype(BF), jnp.exp(total_log), tail)
-    total = jnp.zeros((n_fs, ch, ch), F32)
-    for d in range(n_sp - 2, -1, -1):
-        total = de[d][:, :, None] * total + st[d].astype(F32)
-    entering = incoming + off[:, :, :, None] * total[None]
-    recurrent = (inner_out + jnp.einsum("nthd,nhde->nthe", q_up, entering, precision=HIGH)).reshape(rows, n_fs, ch)
-    square_sum = jnp.sum(recurrent * recurrent, axis=2)
-    rec_act = (recurrent * gain * jax.nn.silu(z_outgate)).astype(BF).transpose(1, 0, 2).reshape(n_fs * rows, ch)
-    sq = jnp.pad(square_sum.T.reshape(n_fs, lanes, 128), ((0, 0), (0, 8 - lanes), (0, 0)))
-
-    zp = z[:, :, (n_w - 1) * ch :]
-    running = jnp.concatenate([rim, zp], axis=1).astype(F32)
-    group_dim = group_weight.shape[1]
-    group = (t * width + f * ch) // group_dim
-    window_total = None
-    for level in range(POOL_GROUPS):
-        stride = 2**level
-        running = running[:, stride:] + running[:, :-stride]
-        now = running[:, running.shape[1] - rows :]
-        window_total = now if level == 0 else jnp.where(group == level, now, window_total)
-    spot = s * rows + jnp.arange(rows, dtype=jnp.int32)
-    counts = jnp.minimum(spot + 1, jnp.left_shift(jnp.int32(2), group)).astype(F32)
-    pooled = (window_total / counts[None, :, None] - zp.astype(F32)).astype(BF).reshape(n_fs * rows, ch)
-
-    n_half = n_sp // n_tp
-    act = jnp.stack([rec_act, pooled])
+    )(z, e_all, forget_gap[None], rec_gain[None])
     out_shape = (n_fs, n_tp, rows // n_tp, n_half * cw)
     (final,) = comm(
         functools.partial(mix_kernel, n_sp, n_fs, n_tp),

time: 135 us -> 123 us (0.911)
  Pallas kernels: 107 us -> 119 us
  local copies, waits for them, and re-layouts: 14.5 us -> 4.34 us
  other arithmetic: 8.47 us -> 0 us
  matrix products: 3.67 us -> 0 us
    pallas_call x1, Pallas kernels: 9.07 us -> 17.9 us  [body(): comm(functools.partial(state_kernel, n_sp, group_weight.shape[1]), [((2,...]
    dot_general x4 -> x0, matrix products: 3.67 us -> none  [the longest x1 1.33 us: body(): jnp.einsum('nthd,nhde->nthe', q_up, entering, precision=HIGH)]
    slice x7 -> x0, local copies, waits for them, and re-layouts: 2.81 us -> none  [the longest x1 1.31 us: body(): tail = z[:, rows - reach:, (n_w - 1) * ch:]]
    pallas_call x1, Pallas kernels: 43.8 us -> 46.5 us  [body(): comm(functools.partial(mix_kernel, n_sp, n_fs, n_tp), [(out_shape, BF)],...]
    mul x4 -> x0, other arithmetic: 2.69 us -> none  [the longest x1 1.3 us: body(): entering = incoming + off[:, :, :, None] * total[None]]
    convert_element_type x4 -> x0, other arithmetic: 2.35 us -> none  [the longest x1 1.31 us: body(): (window_total / counts[None, :, None] - zp.astype(F32)).astype(BF)]
    unnamed x6 -> x0, local copies, waits for them, and re-layouts: 2.23 us -> none
    transpose x2 -> x0, local copies, waits for them, and re-layouts: 1.76 us -> none  [the longest x1 1.59 us: body(): zf = z.astype(F32).transpose(1, 0, 2).reshape(rows, n_fs, n_w, ch)]
where the time goes in v4:
time: 123 us
  Pallas kernels  119 us (97%)
  local copies, waits for them, and re-layouts  4.34 us (4%)
    pallas_call x1, Pallas kernels, body(): comm(functools.partial(project_kernel, n_sp, n_fs, n_tp), [((n_fs, rows,...  54.3 us
    pallas_call x1, Pallas kernels, body(): comm(functools.partial(mix_kernel, n_sp, n_fs, n_tp), [(out_shape, BF)],...  46.5 us
    pallas_call x1, Pallas kernels, body(): comm(functools.partial(state_kernel, n_sp, group_weight.shape[1]), [((2,...  17.9 us

profile of v4, /device:TPU:1, one launch (start us, length us, event | category | flops | bytes accessed | tf_op | source)
XLA Modules:
  0.0 123.1 jit_solution(9740197032905233106)
XLA Ops:
  0.0 0.7 reshape.9
  0.7 0.6 pad.4.extra
  1.3 54.3 %project.1 = (bf16[4,256,640]{2,1,0:T(8,128)(2,1)}, f32[4,8,128]{2,1,0:T(8,128)}, bf16[1024,128]{1,0:T(8,128)(2,1)}) custom-call(bf16[256,1024]{1,0:T(8,128)(2,1)} %bitcast.12, bf16[128,512]{1,0:T(8,128)(2,1)} %wq.1, bf16[128,512]{1,0:T(8,128)(2,1)} %wf.1, bf16[128,512]{1,0:T(8,128)(2,1)} %wi.1, bf16[128,512]{1,0:T(8,128)(2,1)} %wo.1, bf16[128,512]{1,0:T(8,128)(2,1)} %wp.1, ...), custom_call_target="tpu_custom_call" | custom-call | tf_op jit(solution)/shard_map/project/pallas_call | solution.py:545
  55.6 17.9 %state.1 = (bf16[2,1024,128]{2,1,0:T(8,128)(2,1)}, f32[4,8,128]{2,1,0:T(8,128)}) custom-call(bf16[4,256,640]{2,1,0:T(8,128)(2,1)} %get-tuple-element.10.z, f32[4,8,128]{2,1,0:T(8,128)} %get-tuple-element.11.e_all, f32[1,512]{1,0:T(1,128)} %bitcast.16, f32[1,512]{1,0:T(1,128)} %bitcast.17), custom_call_target="tpu_custom_call" | custom-call | tf_op jit(solution)/shard_map/state/pallas_call | solution.py:560
  73.5 46.5 %mix.1 = bf16[4,2,128,256]{3,2,1,0:T(8,128)(2,1)} custom-call(bf16[2,1024,128]{2,1,0:T(8,128)(2,1)} %get-tuple-element.12.act, f32[4,8,128]{2,1,0:T(8,128)} %get-tuple-element.13.sq, bf16[1024,128]{1,0:T(8,128)(2,1)} %get-tuple-element.14.ow), custom_call_target="tpu_custom_call" | custom-call | tf_op jit(solution)/shard_map/mix/pallas_call | solution.py:573
  120.0 1.2 reshape.10
  121.2 0.7 copy.15
  121.9 1.2 reshape.11

commit v5 on v4

--- a/solution.py
+++ b/solution.py
@@ -341,8 +341,8 @@
 
 
 def mix_kernel(
-    n_sp, n_fs, n_tp, act, sq, ow, out,
-    acts, sq_all, ow_all, relay_buf, wbuf, part,
+    n_sp, n_fs, n_tp, act, sq, ow, final,
+    out, acts, sq_all, ow_all, relay_buf, wbuf, part,
     a_send, a_recv, f_send, d_send, d_recv, q_send, q_recv,
     up_send, down_send, o_recv, od_send, od_recv, m_send, m_recv,
 ):
@@ -506,6 +506,11 @@
             rcopy(here, here, m_send.at[g, u], m_recv.at[g, u], other).wait_recv()
     here = out.at[f, 1 - t]
     rcopy(here, here, m_send.at[f, 1 - t], m_recv.at[f, 1 - t], other).wait_recv()
+    for u in range(n_tp):
+        for i in range(n_half):
+            for g in range(n_fs):
+                lo = ((u * n_half + i) * n_fs + g) * cw
+                final[:, lo : lo + cw] = out[g, u, :, i * cw : (i + 1) * cw]
 
 
 def vmem(count):
@@ -572,9 +577,9 @@
     out_shape = (n_fs, n_tp, rows // n_tp, n_half * cw)
     (final,) = comm(
         functools.partial(mix_kernel, n_sp, n_fs, n_tp),
-        [(out_shape, BF)],
+        [((rows // n_tp, n_tp * n_half * n_fs * cw), BF)],
         [
-            pltpu.VMEM((n_tp, n_fs) + act.shape, BF), pltpu.VMEM((n_tp, n_fs) + sq.shape, F32),
+            pltpu.VMEM(out_shape, BF), pltpu.VMEM((n_tp, n_fs) + act.shape, BF), pltpu.VMEM((n_tp, n_fs) + sq.shape, F32),
             pltpu.VMEM((n_half, n_tp) + ow.shape, BF), pltpu.VMEM((n_sp,) + ow.shape, BF),
             pltpu.VMEM((2, n_tp * width, n_half * cw), BF), pltpu.VMEM(out_shape, BF),
             dma(2, 2), dma(n_fs, 2), dma(2), dma(n_fs, 2), dma(n_fs, 2), dma(n_fs, n_tp), dma(n_tp, n_fs),
@@ -582,8 +587,7 @@
         ],
         3, "mix",
     )(act, sq, ow)
-    final = final.reshape(n_fs, n_tp, rows // n_tp, n_half, cw).transpose(2, 1, 3, 0, 4)
-    return final.reshape(1, rows // n_tp, n_tp * n_half * n_fs * cw)
+    return final[None]
 
 
 def solution(mesh):

time: 123 us -> 122 us (level)
    reshape x2 -> x0, local copies, waits for them, and re-layouts: 2.35 us -> none  [the longest x1 1.18 us: body(): return final.reshape(1, rows // n_tp, n_tp * n_half * n_fs * cw)]
    unnamed x0 -> x1, local copies, waits for them, and re-layouts: none -> 1.88 us
where the time goes in v5:
time: 122 us
  Pallas kernels  119 us (98%)
  local copies, waits for them, and re-layouts  3.19 us (3%)
    pallas_call x1, Pallas kernels, body(): comm(functools.partial(project_kernel, n_sp, n_fs, n_tp), [((n_fs, rows,...  54.3 us
    pallas_call x1, Pallas kernels, body(): comm(functools.partial(mix_kernel, n_sp, n_fs, n_tp), [((rows // n_tp, n_...  46.7 us
    pallas_call x1, Pallas kernels, body(): comm(functools.partial(state_kernel, n_sp, group_weight.shape[1]), [((2,...  17.9 us

profile of v5, /device:TPU:1, one launch (start us, length us, event | category | flops | bytes accessed | tf_op | source)
XLA Modules:
  0.0 122.1 jit_solution(12853854571828597920)
XLA Ops:
  0.0 0.7 reshape.3
  0.7 0.6 pad.4.extra
  1.3 54.3 %project.1 = (bf16[4,256,640]{2,1,0:T(8,128)(2,1)}, f32[4,8,128]{2,1,0:T(8,128)}, bf16[1024,128]{1,0:T(8,128)(2,1)}) custom-call(bf16[256,1024]{1,0:T(8,128)(2,1)} %bitcast.10, bf16[128,512]{1,0:T(8,128)(2,1)} %wq.1, bf16[128,512]{1,0:T(8,128)(2,1)} %wf.1, bf16[128,512]{1,0:T(8,128)(2,1)} %wi.1, bf16[128,512]{1,0:T(8,128)(2,1)} %wo.1, bf16[128,512]{1,0:T(8,128)(2,1)} %wp.1, ...), custom_call_target="tpu_custom_call" | custom-call | tf_op jit(solution)/shard_map/project/pallas_call | solution.py:550
  55.6 17.9 %state.1 = (bf16[2,1024,128]{2,1,0:T(8,128)(2,1)}, f32[4,8,128]{2,1,0:T(8,128)}) custom-call(bf16[4,256,640]{2,1,0:T(8,128)(2,1)} %get-tuple-element.10.z, f32[4,8,128]{2,1,0:T(8,128)} %get-tuple-element.11.e_all, f32[1,512]{1,0:T(1,128)} %bitcast.14, f32[1,512]{1,0:T(1,128)} %bitcast.15), custom_call_target="tpu_custom_call" | custom-call | tf_op jit(solution)/shard_map/state/pallas_call | solution.py:565
  73.5 46.7 %mix.1 = bf16[128,2048]{1,0:T(8,128)(2,1)} custom-call(bf16[2,1024,128]{2,1,0:T(8,128)(2,1)} %get-tuple-element.12.act, f32[4,8,128]{2,1,0:T(8,128)} %get-tuple-element.13.sq, bf16[1024,128]{1,0:T(8,128)(2,1)} %get-tuple-element.14.ow), custom_call_target="tpu_custom_call" | custom-call | tf_op jit(solution)/shard_map/mix/pallas_call | solution.py:578
  120.2 1.9 %copy.16 = bf16[1,128,2048]{2,1,0:T(8,128)(2,1)} copy(bf16[1,128,2048]{2,1,0:T(8,128)(2,1)} %bitcast.9) | data formatting | bytes 1048576
